TPU v7x, 512 devices: a whole 4x8x8 slice. The times are simulated.
512 devices in a mesh: gr: 2 (over z_hi), fs: 32 (over z_lo, y), tp: 8 (over x, core).
Axes of the slice: x: 4, y: 8, z: 8 (z_hi: 2, z_lo: 4; z = z_hi * 4 + z_lo), core: 2. Of those that a mesh axis runs over, the one named last changes fastest.
Arguments:
- prompt: bfloat16 [16, 256, 2048], P(('gr', 'tp')), as said below
- norm_gain: float32 [2, 2048], P(None, 'fs'), may hold values from 0.1 to 1.9
- gate_weight: float32 [2, 2048, 4096], P(None, 'fs', ('gr', 'tp')), may hold values from -0.125 to 0.125
- up_weight: float32 [2, 2048, 4096], P(None, 'fs', ('gr', 'tp')), may hold values from -0.125 to 0.125
- down_weight: float32 [2, 4096, 2048], P(None, 'fs', ('gr', 'tp')), may hold values from -0.09375 to 0.09375
Outputs:
- gate_sampler: bfloat16 [2, 2048, 4096], P(None, None, 'fs')
- up_sampler: bfloat16 [2, 2048, 4096], P(None, None, 'fs')
- down_sampler: bfloat16 [2, 4096, 2048], P(None, 'fs')
- mixed: bfloat16 [16, 256, 2048], P(('gr', 'tp'))
Inputs may be any that keep to these rules, and one draw needn't show every extreme that they name: prompt features have scales that differ from feature to feature.
All inputs are finite; a program needn't handle non-finite values.
Results may differ from a plain program's by a relative error of at most 0.0043.
Values may be sent and summed in bfloat16 or wider, within the bound.
No kernel may reach another device: no remote copies, remote signals or barrier semaphores. Data moves between devices by JAX's collectives and lax.ppermute only.
A program may use at most 64 MiB of HBM per device.

v0:
```python
import jax
import jax.numpy as jnp
from jax import lax
from jax.experimental import pallas as pl
from jax.experimental.pallas import tpu as pltpu
from jax.sharding import Mesh
from jax.sharding import PartitionSpec as P


norm_eps = 1e-06
bf16 = jnp.bfloat16
f32 = jnp.float32

AXES = ("gr", "zl", "yh", "yl", "x", "core")
SIZES = (2, 4, 4, 2, 4, 2)
FS = ("zl", "yh", "yl")
GT = ("gr", "x", "core")
SWAP = [(0, 1), (1, 0)]


def device(gr, fs, tp):
    return gr * 256 + fs * 8 + tp


def everyone():
    return [(gr, fs, tp) for gr in range(2) for fs in range(32) for tp in range(8)]


def weight_moves():
    moves = []
    for gr, fs, tp in everyone():
        to = device(fs >> 4, 2 * (8 * gr + tp) + (fs & 1), (fs >> 1) & 7)
        moves.append((device(gr, fs, tp), to))
    return moves


def in_vmem(value):
    return pltpu.with_memory_space_constraint(value, pltpu.VMEM)


def kernel(body, outs, scratch=()):
    here = pl.BlockSpec(memory_space=pltpu.VMEM)

    def call(*args):
        return pl.pallas_call(
            body,
            in_specs=[here] * len(args),
            out_specs=tuple(here for _ in outs),
            out_shape=tuple(pltpu.VMEM(shape, bf16) for shape in outs),
            scratch_shapes=[pltpu.VMEM(shape, bf16) for shape in scratch],
            compiler_params=pltpu.CompilerParams(vmem_limit_bytes=24 << 20),
        )(*[in_vmem(a) for a in args])

    return call


def in_order(first, second, swapped):
    return jnp.where(swapped, second, first), jnp.where(swapped, first, second)


def to_everyone(value, axes, count):
    return lax.all_to_all(
        jnp.broadcast_to(value[None], (count, *value.shape)), axes, 0, 0, tiled=True
    )


def layer_call(late, normed, own, other, outputs):
    layer = 1 if late else 0

    def body(normed, own, other, *refs):
        gates, ups, serveds, part, wide, down, gate, up, served, done = refs[3 * layer :]
        core = lax.axis_index("core") == 0
        even = lax.axis_index("yl") == 0
        for k in range(4):
            x = lax.axis_index("x") ^ k if late else k
            for b in range(2):
                for s in range(3):
                    mn = own[k, b, 128 * s : 128 * s + 128]
                    ot = other[k, b, 128 * s : 128 * s + 128]
                    for c in range(2):
                        line = jnp.where(core, mn, ot) if c == 0 else jnp.where(core, ot, mn)
                        at = 128 * c + 64 * b
                        if s < 2:
                            wide[s, x, at : at + 64, :256] = line[:64]
                            wide[s, x, at : at + 64, 256:] = line[64:]
                        else:
                            for g in range(2):
                                down[g, x, 128 * b : 128 * b + 128, 128 * c : 128 * c + 128] = line[
                                    :, 128 * g : 128 * g + 128
                                ]
        act = jnp.zeros((128, 512), f32)
        for s in range(2):
            for x in range(4):
                at = 1024 * s + 256 * x
                block = wide[s, x]
                gate[at : at + 256] = jnp.where(even, block[:, :128], block[:, 128:256])
                up[at : at + 256] = jnp.where(even, block[:, 256:384], block[:, 384:])
        for g in range(2):
            for x in range(4):
                block = down[g, x]
                at = 1024 * g + 256 * x
                served[:, at : at + 256] = jnp.where(even, block[:128], block[128:])
        copies = [
            pltpu.make_async_copy(a, b.at[layer], done.at[i])
            for i, (a, b) in enumerate(((gate, gates), (up, ups), (served, serveds)))
        ]
        for copy in copies:
            copy.start()
        for s in range(2):
            for x in range(4):
                at = 1024 * s + 256 * x
                act = act + jnp.dot(
                    normed[:, at : at + 256], wide[s, x], preferred_element_type=f32
                )
        gate_act, up_act = act[:, :256], act[:, 256:]
        hidden = (gate_act / (1.0 + jnp.exp(-gate_act)) * up_act).astype(bf16)
        for g in range(2):
            for x in range(4):
                at = 1024 * g + 256 * x
                out = jnp.dot(hidden, down[g, x], preferred_element_type=f32)
                part[:, at : at + 256] = out.astype(bf16)
        for copy in copies:
            copy.wait()

    here = pl.BlockSpec(memory_space=pltpu.VMEM)
    there = pl.BlockSpec(memory_space=pl.ANY)
    scratch = ((2, 4, 256, 512), (2, 4, 256, 256), (2048, 128), (2048, 128), (128, 2048))
    shapes = ((2, 2048, 128), (2, 2048, 128), (2, 128, 2048))
    return pl.pallas_call(
        body,
        in_specs=[here] * 3 + [there] * len(outputs),
        out_specs=(there, there, there, here),
        out_shape=(
            *(jax.ShapeDtypeStruct(shape, bf16) for shape in shapes),
            pltpu.VMEM((128, 2048), bf16),
        ),
        input_output_aliases={3 + i: i for i in range(len(outputs))},
        scratch_shapes=[
            *(pltpu.VMEM(shape, bf16) for shape in scratch),
            pltpu.SemaphoreType.DMA((3,)),
        ],
        compiler_params=pltpu.CompilerParams(vmem_limit_bytes=24 << 20),
        name="late_layer" if late else "early_layer",
    )(in_vmem(normed), in_vmem(own), in_vmem(other), *outputs)


def normalised(value):
    mean = jnp.sum(value * value, axis=1, keepdims=True) * (1.0 / 2048)
    return (value * lax.rsqrt(mean + norm_eps)).astype(bf16)


def norm_call(stream):
    def body(stream, out):
        out[...] = normalised(stream[...].astype(f32))

    return kernel(body, (stream.shape,))(stream)[0]


def fold_call(last, parts, mine):
    count = 32 if last else 16

    def body(parts, mine, sends, total):
        value = mine[...]
        summed = parts[0].astype(f32)
        for i in range(1, 16):
            summed = summed + parts[i].astype(f32)
        value = value + 0.5 * summed
        total[...] = value
        sent = value.astype(bf16) if last else normalised(value)
        for i in range(count):
            sends[i] = sent

    here = pl.BlockSpec(memory_space=pltpu.VMEM)
    return pl.pallas_call(
        body,
        in_specs=[here, here],
        out_specs=(here, here),
        out_shape=(pltpu.VMEM((count, 8, 2048), bf16), pltpu.VMEM((8, 2048), f32)),
        compiler_params=pltpu.CompilerParams(vmem_limit_bytes=24 << 20),
        name="fold",
    )(in_vmem(parts), in_vmem(mine))


def step(prompt, norm_gain, gate_weight, up_weight, down_weight):
    gain = norm_gain[:, :, None]
    gate = (gain * gate_weight).astype(bf16)
    up = (gain * up_weight).astype(bf16)
    high = lax.axis_index("gr") == 1
    moved = []
    for layer in range(2):
        block = jnp.concatenate([gate[layer], up[layer]], axis=0)
        moved.append(lax.ppermute(block, AXES, weight_moves()))
    down = down_weight.astype(bf16)

    def with_down(layer):
        packed = jnp.concatenate([down[layer, :64], down[layer, 64:]], axis=1)
        return jnp.concatenate([moved[layer], packed], axis=0)

    def unpacked(low, top):
        upper = jnp.concatenate([low[128:, :128], top[128:, :128]], axis=1)
        lower = jnp.concatenate([low[128:, 128:], top[128:, 128:]], axis=1)
        return jnp.concatenate([low[:128], top[:128], upper, lower], axis=0)

    both = with_down(0)
    across = lax.ppermute(both, "gr", SWAP)
    block = unpacked(*in_order(both, across, high))

    own = to_everyone(block, ("x", "yl"), 8)
    own, moved[1] = lax.optimization_barrier((own, moved[1]))
    both = with_down(1)
    across = lax.ppermute(both, "gr", SWAP)
    block = unpacked(*in_order(both, across, high))
    yl = lax.axis_index("yl")
    came = lax.ppermute(block, "yl", SWAP)
    other = lax.ppermute(own, "core", SWAP)
    pair = jnp.stack(in_order(block, came, yl == 1))
    late = [lax.ppermute(pair, "x", [(x, x ^ k) for x in range(4)]) for k in (1, 2, 3)]
    late = jnp.stack([pair, *late])
    late_other = lax.ppermute(late, "core", SWAP)

    half = lax.dynamic_slice_in_dim(prompt[0], yl * 128, 128, 0)
    mine = lax.dynamic_slice_in_dim(half, lax.axis_index(("zl", "yh")) * 8, 8, 0).astype(f32)
    normed = norm_call(half)
    early = [a.reshape(4, 2, 384, 256) for a in (own, other)]
    outputs = ()
    for layer in range(2):
        pieces = (late, late_other) if layer else early
        *outputs, part = layer_call(layer == 1, normed, *pieces, outputs)
        parts = lax.all_to_all(part.reshape(16, 8, 2048), ("zl", "yh"), 0, 0, tiled=True)
        sends, mine = fold_call(layer == 1, parts, mine)
        axes = ("yl", "zl", "yh") if layer else ("zl", "yh")
        normed = lax.all_to_all(sends, axes, 0, 0, tiled=True).reshape(-1, 2048)
    return *outputs, normed.reshape(prompt.shape)


def solution(mesh):
    fine = Mesh(mesh.devices.reshape(SIZES), AXES)
    in_specs = (P(GT, None, None), P(None, FS), P(None, FS, GT), P(None, FS, GT), P(None, FS, GT))
    out_specs = (P(None, None, FS), P(None, None, FS), P(None, FS, None), P(GT, None, None))
    return jax.shard_map(step, mesh=fine, in_specs=in_specs, out_specs=out_specs, check_vma=False)
```

profile of v0, /device:TPU:18, one launch (start us, length us, event | category | flops | bytes accessed | tf_op | source)
XLA Modules:
  0.0 205.6 jit_solution(16986646446428655347)
XLA Ops:
  0.6 1.1 multiply_convert_fusion.1
  1.7 5.1 %collective-permute-start = (bf16[128,256]{1,0:T(8,128)(2,1)S(1)}, bf16[128,256]{1,0:T(8,128)(2,1)S(1)}, u32[]{:S(2)}, u32[]{:S(2)}) collective-permute-start(bf16[128,256]{1,0:T(8,128)(2,1)S(1)} %pad_maximum_fusion.2), channel_id=1, source_target_pairs={{0,0},{1,16},{2,32},{3,48},{4,64},{5,80},{6,96},{7,112},{8,8},{9,2... | collective-permute-start | bytes 196616 | tf_op jit(solution)/shard_map/ppermute | solution.py:192
  6.9 0.9 convert_element_type.16
  7.8 2.5 %collective-permute-done = bf16[128,256]{1,0:T(8,128)(2,1)S(1)} collective-permute-done((bf16[128,256]{1,0:T(8,128)(2,1)S(1)}, bf16[128,256]{1,0:T(8,128)(2,1)S(1)}, u32[]{:S(2)}, u32[]{:S(2)}) %collective-permute-start) | collective-permute-done | bytes 65568 | tf_op jit(solution)/shard_map/ppermute | solution.py:192
  10.3 15.3 %collective-permute-start.1 = (bf16[192,256]{1,0:T(8,128)(2,1)S(1)}, bf16[192,256]{1,0:T(8,128)(2,1)S(1)}, u32[]{:S(2)}, u32[]{:S(2)}) collective-permute-start(bf16[192,256]{1,0:T(8,128)(2,1)S(1)} %maximum_maximum_fusion.2), channel_id=1, source_target_pairs={{0,256},{256,0},{1,257},{257,1},{2,258},{258,2},{3,259},{259,3},{4... | collective-permute-start | bytes 294920 | tf_op jit(solution)/shard_map/ppermute | solution.py:205
  25.6 5.1 %collective-permute-done.1 = bf16[192,256]{1,0:T(8,128)(2,1)S(1)} collective-permute-done((bf16[192,256]{1,0:T(8,128)(2,1)S(1)}, bf16[192,256]{1,0:T(8,128)(2,1)S(1)}, u32[]{:S(2)}, u32[]{:S(2)}) %collective-permute-start.1) | collective-permute-done | bytes 98336 | tf_op jit(solution)/shard_map/ppermute | solution.py:205
  30.9 1.3 broadcast_in_dim.2
  32.2 4.4 %all-to-all-start = ((bf16[8,384,256]{2,1,0:T(8,128)(2,1)}), bf16[8,384,256]{2,1,0:T(8,128)(2,1)S(1)}, u32[]{:S(2)}, u32[]{:S(2)}) async-start(bf16[8,384,256]{2,1,0:T(8,128)(2,1)} %broadcast_in_dim.2), calls=%async_computation | async-start | bytes 3145728 | tf_op jit(solution)/shard_map/all_to_all | solution.py:62
  36.6 2.0 collective-permute-start.2
  38.6 19.9 %collective-permute-done.2 = bf16[128,256]{1,0:T(8,128)(2,1)S(1)} collective-permute-done((bf16[128,256]{1,0:T(8,128)(2,1)S(1)}, bf16[128,256]{1,0:T(8,128)(2,1)S(1)}, u32[]{:S(2)}, u32[]{:S(2)}) %collective-permute-start.2) | collective-permute-done | bytes 65568 | tf_op jit(solution)/shard_map/ppermute | solution.py:192
  59.2 7.9 %collective-permute-start.4 = (bf16[192,256]{1,0:T(8,128)(2,1)S(1)}, bf16[192,256]{1,0:T(8,128)(2,1)S(1)}, u32[]{:S(2)}, u32[]{:S(2)}) collective-permute-start(bf16[192,256]{1,0:T(8,128)(2,1)S(1)} %maximum_maximum_fusion.3), channel_id=1, source_target_pairs={{0,256},{256,0},{1,257},{257,1},{2,258},{258,2},{3,259},{259,3},{4... | collective-permute-start | bytes 294920 | tf_op jit(solution)/shard_map/ppermute | solution.py:211
  67.1 1.9 collective-permute-start.3
  69.0 0.9 collective-permute-done.4
  70.0 5.1 %collective-permute-start.5 = (bf16[384,256]{1,0:T(8,128)(2,1)S(1)}, bf16[384,256]{1,0:T(8,128)(2,1)}, u32[]{:S(2)}, u32[]{:S(2)}) collective-permute-start(bf16[384,256]{1,0:T(8,128)(2,1)S(1)} %maximum_maximum_fusion.1), channel_id=1, source_target_pairs={{0,8},{8,0},{1,9},{9,1},{2,10},{10,2},{3,11},{11,3},{4,12},{12,4},... | collective-permute-start | bytes 589832 | tf_op jit(solution)/shard_map/ppermute | solution.py:214
  75.1 5.0 %collective-permute-done.5 = bf16[384,256]{1,0:T(8,128)(2,1)} collective-permute-done((bf16[384,256]{1,0:T(8,128)(2,1)S(1)}, bf16[384,256]{1,0:T(8,128)(2,1)}, u32[]{:S(2)}, u32[]{:S(2)}) %collective-permute-start.5) | collective-permute-done | bytes 196640 | tf_op jit(solution)/shard_map/ppermute | solution.py:214
  80.1 1.0 select_bitcast_fusion.1
  81.9 1.9 collective-permute-start.7
  83.9 2.9 %collective-permute-start.6 = (bf16[2,384,256]{2,1,0:T(8,128)(2,1)}, bf16[2,384,256]{2,1,0:T(8,128)(2,1)}, u32[]{:S(2)}, u32[]{:S(2)}) collective-permute-start(bf16[2,384,256]{2,1,0:T(8,128)(2,1)} %get-tuple-element.31), channel_id=1, source_target_pairs={{0,2},{2,0},{4,6},{6,4},{1,3},{3,1},{5,7},{7,5},{8,10},{10,8},{12,... | collective-permute-start | bytes 1179656 | tf_op jit(solution)/shard_map/ppermute | solution.py:217
  86.8 5.0 %collective-permute-start.8 = (bf16[2,384,256]{2,1,0:T(8,128)(2,1)}, bf16[2,384,256]{2,1,0:T(8,128)(2,1)}, u32[]{:S(2)}, u32[]{:S(2)}) collective-permute-start(bf16[2,384,256]{2,1,0:T(8,128)(2,1)} %get-tuple-element.31), channel_id=1, source_target_pairs={{0,6},{2,4},{4,2},{6,0},{1,7},{3,5},{5,3},{7,1},{8,14},{10,12},{12... | collective-permute-start | bytes 1179656 | tf_op jit(solution)/shard_map/ppermute | solution.py:217
  92.0 1.6 early_layer.1
  94.4 9.1 %all-to-all-start.1 = ((bf16[16,8,2048]{2,1,0:T(8,128)(2,1)}), bf16[16,8,2048]{2,1,0:T(8,128)(2,1)S(1)}, u32[]{:S(2)}, u32[]{:S(2)}) async-start(bf16[16,8,2048]{2,1,0:T(8,128)(2,1)} %bitcast.39), calls=%async_computation.1 | async-start | bytes 1048576 | tf_op jit(solution)/shard_map/all_to_all | solution.py:229
  104.3 1.4 pad_maximum_fusion.own
  105.8 1.9 collective-permute-start.9
  107.7 0.9 bitcast_convert_fusion.mine
  108.6 12.2 %all-to-all-done.1.parts = bf16[16,8,2048]{2,1,0:T(8,128)(2,1)S(1)} async-done(((bf16[16,8,2048]{2,1,0:T(8,128)(2,1)}), bf16[16,8,2048]{2,1,0:T(8,128)(2,1)S(1)}, u32[]{:S(2)}, u32[]{:S(2)}) %all-to-all-start.1) | async-done | bytes 524320 | tf_op jit(solution)/shard_map/all_to_all | solution.py:229
  120.8 1.0 fold.2
  121.8 5.6 %all-to-all-start.2 = ((bf16[16,8,2048]{2,1,0:T(8,128)(2,1)}), bf16[16,8,2048]{2,1,0:T(8,128)(2,1)S(1)}, u32[]{:S(2)}, u32[]{:S(2)}) async-start(bf16[16,8,2048]{2,1,0:T(8,128)(2,1)} %get-tuple-element.19), calls=%async_computation.2 | async-start | bytes 1048576 | tf_op jit(solution)/shard_map/all_to_all | solution.py:232
  127.3 17.3 %all-to-all-done.2 = bf16[16,8,2048]{2,1,0:T(8,128)(2,1)S(1)} async-done(((bf16[16,8,2048]{2,1,0:T(8,128)(2,1)}), bf16[16,8,2048]{2,1,0:T(8,128)(2,1)S(1)}, u32[]{:S(2)}, u32[]{:S(2)}) %all-to-all-start.2) | async-done | bytes 524320 | tf_op jit(solution)/shard_map/all_to_all | solution.py:232
  144.7 3.5 %late_layer.1 = (bf16[2,2048,128]{2,1,0:T(8,128)(2,1)}, bf16[2,2048,128]{2,1,0:T(8,128)(2,1)}, bf16[2,128,2048]{2,1,0:T(8,128)(2,1)}, bf16[128,2048]{1,0:T(8,128)(2,1)S(1)}) custom-call(bf16[128,2048]{1,0:T(8,128)(2,1)S(1)} %bitcast.37, bf16[4,2,384,256]{3,2,1,0:T(8,128)(2,1)S(1)} %pad_maximum_fusion.own, ...), custom_call_target="tpu_custom_call", output_to_operand_aliasing={{0}: (3, {}), {1}: (4, {}), {2}: (5, {})} | custom-call | tf_op jit(solution)/shard_map/late_layer/pallas_call | solution.py:129
  148.2 22.3 %all_to_all.25.parts = bf16[16,8,2048]{2,1,0:T(8,128)(2,1)S(1)} all-to-all(bf16[16,8,2048]{2,1,0:T(8,128)(2,1)S(1)} %bitcast.40), channel_id=1, replica_groups=mesh['gr'=2,'zl'=4,'yh'=4,'yl'=2,'x'=4,'core'=2] {'zl','yh'}, dimensions={0} | all-to-all | bytes 1048576 | tf_op jit(solution)/shard_map/all_to_all | solution.py:229
  171.2 33.4 %all_to_all.26 = bf16[32,8,2048]{2,1,0:T(8,128)(2,1)S(1)} all-to-all(bf16[32,8,2048]{2,1,0:T(8,128)(2,1)S(1)} %get-tuple-element.29), channel_id=1, replica_groups=mesh['gr'=2,'zl'=4,'yh'=4,'yl'=2,'x'=4,'core'=2] {'yl','zl','yh'}, dimensions={0} | all-to-all | bytes 2097152 | tf_op jit(solution)/shard_map/all_to_all | solution.py:232
  204.6 1.0 copy.16
  (32 shorter events, 4.4 us)
Async XLA Ops:
  1.7 8.6 %collective-permute-start = (bf16[128,256]{1,0:T(8,128)(2,1)S(1)}, bf16[128,256]{1,0:T(8,128)(2,1)S(1)}, u32[]{:S(2)}, u32[]{:S(2)}) collective-permute-start(bf16[128,256]{1,0:T(8,128)(2,1)S(1)} %pad_maximum_fusion.2), channel_id=1, source_target_pairs={{0,0},{1,16},{2,32},{3,48},{4,64},{5,80},{6,96},{7,112},{8,8},{9,2... | collective-permute-start | bytes 196616 | tf_op jit(solution)/shard_map/ppermute | solution.py:192
  10.3 20.4 %collective-permute-start.1 = (bf16[192,256]{1,0:T(8,128)(2,1)S(1)}, bf16[192,256]{1,0:T(8,128)(2,1)S(1)}, u32[]{:S(2)}, u32[]{:S(2)}) collective-permute-start(bf16[192,256]{1,0:T(8,128)(2,1)S(1)} %maximum_maximum_fusion.2), channel_id=1, source_target_pairs={{0,256},{256,0},{1,257},{257,1},{2,258},{258,2},{3,259},{259,3},{4... | collective-permute-start | bytes 294920 | tf_op jit(solution)/shard_map/ppermute | solution.py:205
  32.2 27.0 %all-to-all-start = ((bf16[8,384,256]{2,1,0:T(8,128)(2,1)}), bf16[8,384,256]{2,1,0:T(8,128)(2,1)S(1)}, u32[]{:S(2)}, u32[]{:S(2)}) async-start(bf16[8,384,256]{2,1,0:T(8,128)(2,1)} %broadcast_in_dim.2), calls=%async_computation | async-start | bytes 3145728 | tf_op jit(solution)/shard_map/all_to_all | solution.py:62
  36.6 21.8 %collective-permute-start.2 = (bf16[128,256]{1,0:T(8,128)(2,1)S(1)}, bf16[128,256]{1,0:T(8,128)(2,1)S(1)}, u32[]{:S(2)}, u32[]{:S(2)}) collective-permute-start(bf16[128,256]{1,0:T(8,128)(2,1)S(1)} %pad_maximum_fusion.3), channel_id=1, source_target_pairs={{0,0},{1,16},{2,32},{3,48},{4,64},{5,80},{6,96},{7,112},{8,8},{9,2... | collective-permute-start | bytes 196616 | tf_op jit(solution)/shard_map/ppermute | solution.py:192
  59.2 10.7 %collective-permute-start.4 = (bf16[192,256]{1,0:T(8,128)(2,1)S(1)}, bf16[192,256]{1,0:T(8,128)(2,1)S(1)}, u32[]{:S(2)}, u32[]{:S(2)}) collective-permute-start(bf16[192,256]{1,0:T(8,128)(2,1)S(1)} %maximum_maximum_fusion.3), channel_id=1, source_target_pairs={{0,256},{256,0},{1,257},{257,1},{2,258},{258,2},{3,259},{259,3},{4... | collective-permute-start | bytes 294920 | tf_op jit(solution)/shard_map/ppermute | solution.py:211
  67.1 24.9 %collective-permute-start.3 = (bf16[8,384,256]{2,1,0:T(8,128)(2,1)S(1)}, bf16[8,384,256]{2,1,0:T(8,128)(2,1)S(1)}, u32[]{:S(2)}, u32[]{:S(2)}) collective-permute-start(bf16[8,384,256]{2,1,0:T(8,128)(2,1)S(1)} %all-to-all-done), channel_id=1, source_target_pairs={{0,1},{1,0},{2,3},{3,2},{4,5},{5,4},{6,7},{7,6},{8,9},{9,8},{10,11... | collective-permute-start | bytes 4718600 | tf_op jit(solution)/shard_map/ppermute | solution.py:215
  70.0 10.1 %collective-permute-start.5 = (bf16[384,256]{1,0:T(8,128)(2,1)S(1)}, bf16[384,256]{1,0:T(8,128)(2,1)}, u32[]{:S(2)}, u32[]{:S(2)}) collective-permute-start(bf16[384,256]{1,0:T(8,128)(2,1)S(1)} %maximum_maximum_fusion.1), channel_id=1, source_target_pairs={{0,8},{8,0},{1,9},{9,1},{2,10},{10,2},{3,11},{11,3},{4,12},{12,4},... | collective-permute-start | bytes 589832 | tf_op jit(solution)/shard_map/ppermute | solution.py:214
  75.1 16.6 %copy-start.1 = (bf16[1,256,2048]{2,1,0:T(8,128)(2,1)S(1)}, bf16[1,256,2048]{2,1,0:T(8,128)(2,1)}, u32[]{:S(2)}) copy-start(bf16[1,256,2048]{2,1,0:T(8,128)(2,1)} %param.5) | copy-start | bytes 3145732
  81.9 21.6 %collective-permute-start.7 = (bf16[2,384,256]{2,1,0:T(8,128)(2,1)}, bf16[2,384,256]{2,1,0:T(8,128)(2,1)}, u32[]{:S(2)}, u32[]{:S(2)}) collective-permute-start(bf16[2,384,256]{2,1,0:T(8,128)(2,1)} %get-tuple-element.31), channel_id=1, source_target_pairs={{0,4},{2,6},{4,0},{6,2},{1,5},{3,7},{5,1},{7,3},{8,12},{10,14},{12... | collective-permute-start | bytes 1179656 | tf_op jit(solution)/shard_map/ppermute | solution.py:217
  83.9 19.7 %collective-permute-start.6 = (bf16[2,384,256]{2,1,0:T(8,128)(2,1)}, bf16[2,384,256]{2,1,0:T(8,128)(2,1)}, u32[]{:S(2)}, u32[]{:S(2)}) collective-permute-start(bf16[2,384,256]{2,1,0:T(8,128)(2,1)} %get-tuple-element.31), channel_id=1, source_target_pairs={{0,2},{2,0},{4,6},{6,4},{1,3},{3,1},{5,7},{7,5},{8,10},{10,8},{12,... | collective-permute-start | bytes 1179656 | tf_op jit(solution)/shard_map/ppermute | solution.py:217
  86.8 17.6 %collective-permute-start.8 = (bf16[2,384,256]{2,1,0:T(8,128)(2,1)}, bf16[2,384,256]{2,1,0:T(8,128)(2,1)}, u32[]{:S(2)}, u32[]{:S(2)}) collective-permute-start(bf16[2,384,256]{2,1,0:T(8,128)(2,1)} %get-tuple-element.31), channel_id=1, source_target_pairs={{0,6},{2,4},{4,2},{6,0},{1,7},{3,5},{5,3},{7,1},{8,14},{10,12},{12... | collective-permute-start | bytes 1179656 | tf_op jit(solution)/shard_map/ppermute | solution.py:217
  93.6 0.8 copy-start
  94.4 26.3 %all-to-all-start.1 = ((bf16[16,8,2048]{2,1,0:T(8,128)(2,1)}), bf16[16,8,2048]{2,1,0:T(8,128)(2,1)S(1)}, u32[]{:S(2)}, u32[]{:S(2)}) async-start(bf16[16,8,2048]{2,1,0:T(8,128)(2,1)} %bitcast.39), calls=%async_computation.1 | async-start | bytes 1048576 | tf_op jit(solution)/shard_map/all_to_all | solution.py:229
  105.8 21.6 %collective-permute-start.9 = (bf16[4,2,384,256]{3,2,1,0:T(8,128)(2,1)S(1)}, bf16[4,2,384,256]{3,2,1,0:T(8,128)(2,1)}, u32[]{:S(2)}, u32[]{:S(2)}) collective-permute-start(bf16[4,2,384,256]{3,2,1,0:T(8,128)(2,1)S(1)} %pad_maximum_fusion.own), channel_id=1, source_target_pairs={{0,1},{1,0},{2,3},{3,2},{4,5},{5,4},{6,7},{7,6},{8,9},{9,8},{10,11... | collective-permute-start | bytes 4718600 | tf_op jit(solution)/shard_map/ppermute | solution.py:219
  121.8 22.9 %all-to-all-start.2 = ((bf16[16,8,2048]{2,1,0:T(8,128)(2,1)}), bf16[16,8,2048]{2,1,0:T(8,128)(2,1)S(1)}, u32[]{:S(2)}, u32[]{:S(2)}) async-start(bf16[16,8,2048]{2,1,0:T(8,128)(2,1)} %get-tuple-element.19), calls=%async_computation.2 | async-start | bytes 1048576 | tf_op jit(solution)/shard_map/all_to_all | solution.py:232
where the time goes:
time: 206 us
  starting transfers between devices  68.1 us (33%)
  waiting for transfers between devices  64.4 us (31%)
  blocking collectives  55.7 us (27%)
  Pallas kernels  7.08 us (3%)
  other arithmetic  6.22 us (3%)
  local copies, waits for them, and re-layouts  3.16 us (2%)
    all_to_all x1, blocking collectives, step(): normed = lax.all_to_all(sends, axes, 0, 0, tiled=True).reshape(-1, 2048)  33.4 us
    ppermute x2, starting transfers between devices, step(): across = lax.ppermute(both, 'gr', SWAP)  23.2 us
    ppermute x2, waiting for transfers between devices, step(): moved.append(lax.ppermute(block, AXES, weight_moves()))  22.4 us
    all_to_all x1, blocking collectives, step(): lax.all_to_all(part.reshape(16, 8, 2048), ('zl', 'yh'), 0, 0, tiled=True)  22.3 us
    all_to_all x1, waiting for transfers between devices, step(): normed = lax.all_to_all(sends, axes, 0, 0, tiled=True).reshape(-1, 2048)  17.3 us
    all_to_all x1, waiting for transfers between devices, step(): lax.all_to_all(part.reshape(16, 8, 2048), ('zl', 'yh'), 0, 0, tiled=True)  12.2 us
    ppermute x3, starting transfers between devices, step(): lax.ppermute(pair, 'x', [(x, x ^ k) for x in range(4)])  9.81 us
    all_to_all x1, starting transfers between devices, step(): lax.all_to_all(part.reshape(16, 8, 2048), ('zl', 'yh'), 0, 0, tiled=True)  9.1 us
  transfers between devices with their start and end apart: 13, of which 9 were waited for; matrix products, arithmetic and copies ran while one was open for 3% of the time, Pallas kernels for 1%

commit v1 on v0

--- a/solution.py
+++ b/solution.py
@@ -68,38 +68,43 @@
     layer = 1 if late else 0
 
     def body(normed, own, other, *refs):
-        gates, ups, serveds, part, wide, down, gate, up, served, done = refs[3 * layer :]
-        core = lax.axis_index("core") == 0
+        gates, ups, serveds, part, wide, down, gate, up, served, done, *more = refs[3 * layer :]
+        if late:
+            fetch = pltpu.make_async_copy(other, more[0], done.at[3])
+            fetch.start()
+        core = lax.axis_index("core")
         even = lax.axis_index("yl") == 0
-        for k in range(4):
-            x = lax.axis_index("x") ^ k if late else k
-            for b in range(2):
-                for s in range(3):
-                    mn = own[k, b, 128 * s : 128 * s + 128]
-                    ot = other[k, b, 128 * s : 128 * s + 128]
-                    for c in range(2):
-                        line = jnp.where(core, mn, ot) if c == 0 else jnp.where(core, ot, mn)
-                        at = 128 * c + 64 * b
-                        if s < 2:
-                            wide[s, x, at : at + 64, :256] = line[:64]
-                            wide[s, x, at : at + 64, 256:] = line[64:]
-                        else:
-                            for g in range(2):
-                                down[g, x, 128 * b : 128 * b + 128, 128 * c : 128 * c + 128] = line[
-                                    :, 128 * g : 128 * g + 128
-                                ]
+
+        def place(blocks, c):
+            for k in range(4):
+                x = lax.axis_index("x") ^ k if late else k
+                for b in range(2):
+                    for s in range(2):
+                        line = blocks[k, b, 128 * s : 128 * s + 128]
+                        wide[s, x, c, 64 * b : 64 * b + 64, :256] = line[:64]
+                        wide[s, x, c, 64 * b : 64 * b + 64, 256:] = line[64:]
+                    line = blocks[k, b, 256:384]
+                    for g in range(2):
+                        columns = line[:, 128 * g : 128 * g + 128]
+                        down[g, x, c, 128 * b : 128 * b + 128] = columns
+
+        place(own, core)
+        if late:
+            fetch.wait()
+        place(more[0] if late else other, 1 - core)
         act = jnp.zeros((128, 512), f32)
         for s in range(2):
             for x in range(4):
                 at = 1024 * s + 256 * x
-                block = wide[s, x]
+                block = wide[s, x].reshape(256, 512)
                 gate[at : at + 256] = jnp.where(even, block[:, :128], block[:, 128:256])
                 up[at : at + 256] = jnp.where(even, block[:, 256:384], block[:, 384:])
         for g in range(2):
             for x in range(4):
-                block = down[g, x]
-                at = 1024 * g + 256 * x
-                served[:, at : at + 256] = jnp.where(even, block[:128], block[128:])
+                for c in range(2):
+                    at = 1024 * g + 256 * x + 128 * c
+                    block = down[g, x, c]
+                    served[:, at : at + 128] = jnp.where(even, block[:128], block[128:])
         copies = [
             pltpu.make_async_copy(a, b.at[layer], done.at[i])
             for i, (a, b) in enumerate(((gate, gates), (up, ups), (served, serveds)))
@@ -109,26 +114,27 @@
         for s in range(2):
             for x in range(4):
                 at = 1024 * s + 256 * x
-                act = act + jnp.dot(
-                    normed[:, at : at + 256], wide[s, x], preferred_element_type=f32
-                )
+                block = wide[s, x].reshape(256, 512)
+                act = act + jnp.dot(normed[:, at : at + 256], block, preferred_element_type=f32)
         gate_act, up_act = act[:, :256], act[:, 256:]
         hidden = (gate_act / (1.0 + jnp.exp(-gate_act)) * up_act).astype(bf16)
         for g in range(2):
             for x in range(4):
                 at = 1024 * g + 256 * x
-                out = jnp.dot(hidden, down[g, x], preferred_element_type=f32)
+                block = jnp.concatenate([down[g, x, 0], down[g, x, 1]], axis=1)
+                out = jnp.dot(hidden, block, preferred_element_type=f32)
                 part[:, at : at + 256] = out.astype(bf16)
         for copy in copies:
             copy.wait()
 
     here = pl.BlockSpec(memory_space=pltpu.VMEM)
     there = pl.BlockSpec(memory_space=pl.ANY)
-    scratch = ((2, 4, 256, 512), (2, 4, 256, 256), (2048, 128), (2048, 128), (128, 2048))
+    blocks = [pltpu.VMEM(other.shape, bf16)] if late else []
+    scratch = ((2, 4, 2, 128, 512), (2, 4, 2, 256, 128), (2048, 128), (2048, 128), (128, 2048))
     shapes = ((2, 2048, 128), (2, 2048, 128), (2, 128, 2048))
     return pl.pallas_call(
         body,
-        in_specs=[here] * 3 + [there] * len(outputs),
+        in_specs=[here, here, there if late else here] + [there] * len(outputs),
         out_specs=(there, there, there, here),
         out_shape=(
             *(jax.ShapeDtypeStruct(shape, bf16) for shape in shapes),
@@ -137,11 +143,12 @@
         input_output_aliases={3 + i: i for i in range(len(outputs))},
         scratch_shapes=[
             *(pltpu.VMEM(shape, bf16) for shape in scratch),
-            pltpu.SemaphoreType.DMA((3,)),
+            pltpu.SemaphoreType.DMA((4,)),
+            *blocks,
         ],
         compiler_params=pltpu.CompilerParams(vmem_limit_bytes=24 << 20),
         name="late_layer" if late else "early_layer",
-    )(in_vmem(normed), in_vmem(own), in_vmem(other), *outputs)
+    )(in_vmem(normed), in_vmem(own), other if late else in_vmem(other), *outputs)
 
 
 def normalised(value):
@@ -206,12 +213,12 @@
     block = unpacked(*in_order(both, across, high))
 
     own = to_everyone(block, ("x", "yl"), 8)
-    own, moved[1] = lax.optimization_barrier((own, moved[1]))
     both = with_down(1)
     across = lax.ppermute(both, "gr", SWAP)
     block = unpacked(*in_order(both, across, high))
     yl = lax.axis_index("yl")
     came = lax.ppermute(block, "yl", SWAP)
+    own, block = lax.optimization_barrier((own, block))
     other = lax.ppermute(own, "core", SWAP)
     pair = jnp.stack(in_order(block, came, yl == 1))
     late = [lax.ppermute(pair, "x", [(x, x ^ k) for x in range(4)]) for k in (1, 2, 3)]

time: 206 us -> 210 us (1.019)
  the two profiles are of different devices: /device:TPU:18 before, /device:TPU:16 now
where the time goes in v1:
time: 210 us; the launch traced here: 209 us
  starting transfers between devices  82.1 us (39%)
  blocking collectives  56.5 us (27%)
  waiting for transfers between devices  53.8 us (26%)
  Pallas kernels  7.49 us (4%)
  other arithmetic  5.26 us (3%)
  local copies, waits for them, and re-layouts  3.16 us (2%)
    all_to_all x1, blocking collectives, step(): normed = lax.all_to_all(sends, axes, 0, 0, tiled=True).reshape(-1, 2048)  33.7 us
    ppermute x2, starting transfers between devices, step(): across = lax.ppermute(both, 'gr', SWAP)  24.3 us
    all_to_all x1, blocking collectives, step(): lax.all_to_all(part.reshape(16, 8, 2048), ('zl', 'yh'), 0, 0, tiled=True)  22.8 us
    all_to_all x1, waiting for transfers between devices, step(): normed = lax.all_to_all(sends, axes, 0, 0, tiled=True).reshape(-1, 2048)  16.4 us
    ppermute x2, waiting for transfers between devices, step(): moved.append(lax.ppermute(block, AXES, weight_moves()))  14.4 us
    ppermute x3, starting transfers between devices, step(): lax.ppermute(pair, 'x', [(x, x ^ k) for x in range(4)])  13.7 us
    all_to_all x1, waiting for transfers between devices, step(): lax.all_to_all(part.reshape(16, 8, 2048), ('zl', 'yh'), 0, 0, tiled=True)  12.2 us
    all_to_all x1, starting transfers between devices, step(): lax.all_to_all(part.reshape(16, 8, 2048), ('zl', 'yh'), 0, 0, tiled=True)  11.2 us
  transfers between devices with their start and end apart: 13, of which 7 were waited for; matrix products, arithmetic and copies ran while one was open for 2% of the time, Pallas kernels for 2%

profile of v1, /device:TPU:16, one launch (start us, length us, event | category | flops | bytes accessed | tf_op | source)
XLA Modules:
  0.0 209.3 jit_solution(11837947483341273596)
XLA Ops:
  0.6 1.1 multiply_convert_fusion.1
  1.7 1.9 collective-permute-start
  3.7 0.9 convert_element_type.16
  4.6 3.7 %collective-permute-done = bf16[128,256]{1,0:T(8,128)(2,1)S(1)} collective-permute-done((bf16[128,256]{1,0:T(8,128)(2,1)S(1)}, bf16[128,256]{1,0:T(8,128)(2,1)S(1)}, u32[]{:S(2)}, u32[]{:S(2)}) %collective-permute-start) | collective-permute-done | bytes 65568 | tf_op jit(solution)/shard_map/ppermute | solution.py:199
  8.3 13.9 %collective-permute-start.1 = (bf16[192,256]{1,0:T(8,128)(2,1)S(1)}, bf16[192,256]{1,0:T(8,128)(2,1)S(1)}, u32[]{:S(2)}, u32[]{:S(2)}) collective-permute-start(bf16[192,256]{1,0:T(8,128)(2,1)S(1)} %maximum_maximum_fusion.2), channel_id=1, source_target_pairs={{0,256},{256,0},{1,257},{257,1},{2,258},{258,2},{3,259},{259,3},{4... | collective-permute-start | bytes 294920 | tf_op jit(solution)/shard_map/ppermute | solution.py:212
  22.2 2.6 %collective-permute-done.1 = bf16[192,256]{1,0:T(8,128)(2,1)S(1)} collective-permute-done((bf16[192,256]{1,0:T(8,128)(2,1)S(1)}, bf16[192,256]{1,0:T(8,128)(2,1)S(1)}, u32[]{:S(2)}, u32[]{:S(2)}) %collective-permute-start.1) | collective-permute-done | bytes 98336 | tf_op jit(solution)/shard_map/ppermute | solution.py:212
  25.0 1.3 broadcast_in_dim.2
  26.3 9.8 %all-to-all-start = ((bf16[8,384,256]{2,1,0:T(8,128)(2,1)}), bf16[8,384,256]{2,1,0:T(8,128)(2,1)S(1)}, u32[]{:S(2)}, u32[]{:S(2)}) async-start(bf16[8,384,256]{2,1,0:T(8,128)(2,1)} %broadcast_in_dim.2), calls=%async_computation | async-start | bytes 3145728 | tf_op jit(solution)/shard_map/all_to_all | solution.py:62
  36.1 1.9 collective-permute-start.2
  38.0 10.7 %collective-permute-done.2 = bf16[128,256]{1,0:T(8,128)(2,1)S(1)} collective-permute-done((bf16[128,256]{1,0:T(8,128)(2,1)S(1)}, bf16[128,256]{1,0:T(8,128)(2,1)S(1)}, u32[]{:S(2)}, u32[]{:S(2)}) %collective-permute-start.2) | collective-permute-done | bytes 65568 | tf_op jit(solution)/shard_map/ppermute | solution.py:199
  48.7 10.4 %collective-permute-start.3 = (bf16[192,256]{1,0:T(8,128)(2,1)S(1)}, bf16[192,256]{1,0:T(8,128)(2,1)S(1)}, u32[]{:S(2)}, u32[]{:S(2)}) collective-permute-start(bf16[192,256]{1,0:T(8,128)(2,1)S(1)} %maximum_maximum_fusion.3), channel_id=1, source_target_pairs={{0,256},{256,0},{1,257},{257,1},{2,258},{258,2},{3,259},{259,3},{4... | collective-permute-start | bytes 294920 | tf_op jit(solution)/shard_map/ppermute | solution.py:217
  59.2 2.6 %collective-permute-done.3 = bf16[192,256]{1,0:T(8,128)(2,1)S(1)} collective-permute-done((bf16[192,256]{1,0:T(8,128)(2,1)S(1)}, bf16[192,256]{1,0:T(8,128)(2,1)S(1)}, u32[]{:S(2)}, u32[]{:S(2)}) %collective-permute-start.3) | collective-permute-done | bytes 98336 | tf_op jit(solution)/shard_map/ppermute | solution.py:217
  61.9 1.9 collective-permute-start.4
  63.8 10.1 %collective-permute-start.5 = (bf16[384,256]{1,0:T(8,128)(2,1)S(1)}, bf16[384,256]{1,0:T(8,128)(2,1)S(1)}, u32[]{:S(2)}, u32[]{:S(2)}) collective-permute-start(bf16[384,256]{1,0:T(8,128)(2,1)S(1)} %maximum_maximum_fusion.1), channel_id=1, source_target_pairs={{0,8},{8,0},{1,9},{9,1},{2,10},{10,2},{3,11},{11,3},{4,12},{12,4},... | collective-permute-start | bytes 589832 | tf_op jit(solution)/shard_map/ppermute | solution.py:220
  73.9 5.5 %collective-permute-done.5 = bf16[384,256]{1,0:T(8,128)(2,1)S(1)} collective-permute-done((bf16[384,256]{1,0:T(8,128)(2,1)S(1)}, bf16[384,256]{1,0:T(8,128)(2,1)S(1)}, u32[]{:S(2)}, u32[]{:S(2)}) %collective-permute-start.5) | collective-permute-done | bytes 196640 | tf_op jit(solution)/shard_map/ppermute | solution.py:220
  79.5 0.8 fusion
  80.3 4.9 %collective-permute-start.7 = (bf16[2,384,256]{2,1,0:T(8,128)(2,1)}, bf16[2,384,256]{2,1,0:T(8,128)(2,1)}, u32[]{:S(2)}, u32[]{:S(2)}) collective-permute-start(bf16[2,384,256]{2,1,0:T(8,128)(2,1)} %get-tuple-element.31), channel_id=1, source_target_pairs={{0,4},{2,6},{4,0},{6,2},{1,5},{3,7},{5,1},{7,3},{8,12},{10,14},{12... | collective-permute-start | bytes 1179656 | tf_op jit(solution)/shard_map/ppermute | solution.py:224
  85.2 6.7 %collective-permute-start.6 = (bf16[2,384,256]{2,1,0:T(8,128)(2,1)}, bf16[2,384,256]{2,1,0:T(8,128)(2,1)}, u32[]{:S(2)}, u32[]{:S(2)}) collective-permute-start(bf16[2,384,256]{2,1,0:T(8,128)(2,1)} %get-tuple-element.31), channel_id=1, source_target_pairs={{0,2},{2,0},{4,6},{6,4},{1,3},{3,1},{5,7},{7,5},{8,10},{10,8},{12,... | collective-permute-start | bytes 1179656 | tf_op jit(solution)/shard_map/ppermute | solution.py:224
  91.9 2.1 %collective-permute-start.8 = (bf16[2,384,256]{2,1,0:T(8,128)(2,1)}, bf16[2,384,256]{2,1,0:T(8,128)(2,1)}, u32[]{:S(2)}, u32[]{:S(2)}) collective-permute-start(bf16[2,384,256]{2,1,0:T(8,128)(2,1)} %get-tuple-element.31), channel_id=1, source_target_pairs={{0,6},{2,4},{4,2},{6,0},{1,7},{3,5},{5,3},{7,1},{8,14},{10,12},{12... | collective-permute-start | bytes 1179656 | tf_op jit(solution)/shard_map/ppermute | solution.py:224
  94.3 2.1 early_layer.1
  97.2 11.2 %all-to-all-start.1 = ((bf16[16,8,2048]{2,1,0:T(8,128)(2,1)}), bf16[16,8,2048]{2,1,0:T(8,128)(2,1)S(1)}, u32[]{:S(2)}, u32[]{:S(2)}) async-start(bf16[16,8,2048]{2,1,0:T(8,128)(2,1)} %bitcast.39), calls=%async_computation.1 | async-start | bytes 1048576 | tf_op jit(solution)/shard_map/all_to_all | solution.py:236
  108.4 1.4 pad_maximum_fusion.own
  109.8 1.9 collective-permute-start.9
  111.8 0.9 bitcast_convert_fusion.mine
  112.7 12.2 %all-to-all-done.1.parts = bf16[16,8,2048]{2,1,0:T(8,128)(2,1)S(1)} async-done(((bf16[16,8,2048]{2,1,0:T(8,128)(2,1)}), bf16[16,8,2048]{2,1,0:T(8,128)(2,1)S(1)}, u32[]{:S(2)}, u32[]{:S(2)}) %all-to-all-start.1) | async-done | bytes 524320 | tf_op jit(solution)/shard_map/all_to_all | solution.py:236
  124.9 1.0 fold.2
  125.9 5.3 %all-to-all-start.2 = ((bf16[16,8,2048]{2,1,0:T(8,128)(2,1)}), bf16[16,8,2048]{2,1,0:T(8,128)(2,1)S(1)}, u32[]{:S(2)}, u32[]{:S(2)}) async-start(bf16[16,8,2048]{2,1,0:T(8,128)(2,1)} %get-tuple-element.19), calls=%async_computation.2 | async-start | bytes 1048576 | tf_op jit(solution)/shard_map/all_to_all | solution.py:239
  131.2 16.4 %all-to-all-done.2 = bf16[16,8,2048]{2,1,0:T(8,128)(2,1)S(1)} async-done(((bf16[16,8,2048]{2,1,0:T(8,128)(2,1)}), bf16[16,8,2048]{2,1,0:T(8,128)(2,1)S(1)}, u32[]{:S(2)}, u32[]{:S(2)}) %all-to-all-start.2) | async-done | bytes 524320 | tf_op jit(solution)/shard_map/all_to_all | solution.py:239
  147.6 3.4 %late_layer.1 = (bf16[2,2048,128]{2,1,0:T(8,128)(2,1)}, bf16[2,2048,128]{2,1,0:T(8,128)(2,1)}, bf16[2,128,2048]{2,1,0:T(8,128)(2,1)}, bf16[128,2048]{1,0:T(8,128)(2,1)S(1)}) custom-call(bf16[128,2048]{1,0:T(8,128)(2,1)S(1)} %bitcast.37, bf16[4,2,384,256]{3,2,1,0:T(8,128)(2,1)S(1)} %pad_maximum_fusion.own, ...), custom_call_target="tpu_custom_call", output_to_operand_aliasing={{0}: (3, {}), {1}: (4, {}), {2}: (5, {})} | custom-call | tf_op jit(solution)/shard_map/late_layer/pallas_call | solution.py:135
  151.1 22.8 %all_to_all.25.parts = bf16[16,8,2048]{2,1,0:T(8,128)(2,1)S(1)} all-to-all(bf16[16,8,2048]{2,1,0:T(8,128)(2,1)S(1)} %bitcast.40), channel_id=1, replica_groups=mesh['gr'=2,'zl'=4,'yh'=4,'yl'=2,'x'=4,'core'=2] {'zl','yh'}, dimensions={0} | all-to-all | bytes 1048576 | tf_op jit(solution)/shard_map/all_to_all | solution.py:236
  174.7 33.7 %all_to_all.26 = bf16[32,8,2048]{2,1,0:T(8,128)(2,1)S(1)} all-to-all(bf16[32,8,2048]{2,1,0:T(8,128)(2,1)S(1)} %get-tuple-element.29), channel_id=1, replica_groups=mesh['gr'=2,'zl'=4,'yh'=4,'yl'=2,'x'=4,'core'=2] {'yl','zl','yh'}, dimensions={0} | all-to-all | bytes 2097152 | tf_op jit(solution)/shard_map/all_to_all | solution.py:239
  208.3 1.0 copy.16
  (32 shorter events, 2.1 us)
Async XLA Ops:
  1.7 6.5 %collective-permute-start = (bf16[128,256]{1,0:T(8,128)(2,1)S(1)}, bf16[128,256]{1,0:T(8,128)(2,1)S(1)}, u32[]{:S(2)}, u32[]{:S(2)}) collective-permute-start(bf16[128,256]{1,0:T(8,128)(2,1)S(1)} %pad_maximum_fusion.2), channel_id=1, source_target_pairs={{0,0},{1,16},{2,32},{3,48},{4,64},{5,80},{6,96},{7,112},{8,8},{9,2... | collective-permute-start | bytes 196616 | tf_op jit(solution)/shard_map/ppermute | solution.py:199
  8.3 16.5 %collective-permute-start.1 = (bf16[192,256]{1,0:T(8,128)(2,1)S(1)}, bf16[192,256]{1,0:T(8,128)(2,1)S(1)}, u32[]{:S(2)}, u32[]{:S(2)}) collective-permute-start(bf16[192,256]{1,0:T(8,128)(2,1)S(1)} %maximum_maximum_fusion.2), channel_id=1, source_target_pairs={{0,256},{256,0},{1,257},{257,1},{2,258},{258,2},{3,259},{259,3},{4... | collective-permute-start | bytes 294920 | tf_op jit(solution)/shard_map/ppermute | solution.py:212
  26.3 35.6 %all-to-all-start = ((bf16[8,384,256]{2,1,0:T(8,128)(2,1)}), bf16[8,384,256]{2,1,0:T(8,128)(2,1)S(1)}, u32[]{:S(2)}, u32[]{:S(2)}) async-start(bf16[8,384,256]{2,1,0:T(8,128)(2,1)} %broadcast_in_dim.2), calls=%async_computation | async-start | bytes 3145728 | tf_op jit(solution)/shard_map/all_to_all | solution.py:62
  36.1 12.6 %collective-permute-start.2 = (bf16[128,256]{1,0:T(8,128)(2,1)S(1)}, bf16[128,256]{1,0:T(8,128)(2,1)S(1)}, u32[]{:S(2)}, u32[]{:S(2)}) collective-permute-start(bf16[128,256]{1,0:T(8,128)(2,1)S(1)} %pad_maximum_fusion.3), channel_id=1, source_target_pairs={{0,0},{1,16},{2,32},{3,48},{4,64},{5,80},{6,96},{7,112},{8,8},{9,2... | collective-permute-start | bytes 196616 | tf_op jit(solution)/shard_map/ppermute | solution.py:199
  48.7 13.0 %collective-permute-start.3 = (bf16[192,256]{1,0:T(8,128)(2,1)S(1)}, bf16[192,256]{1,0:T(8,128)(2,1)S(1)}, u32[]{:S(2)}, u32[]{:S(2)}) collective-permute-start(bf16[192,256]{1,0:T(8,128)(2,1)S(1)} %maximum_maximum_fusion.3), channel_id=1, source_target_pairs={{0,256},{256,0},{1,257},{257,1},{2,258},{258,2},{3,259},{259,3},{4... | collective-permute-start | bytes 294920 | tf_op jit(solution)/shard_map/ppermute | solution.py:217
  61.9 32.4 %collective-permute-start.4 = (bf16[8,384,256]{2,1,0:T(8,128)(2,1)S(1)}, bf16[8,384,256]{2,1,0:T(8,128)(2,1)S(1)}, u32[]{:S(2)}, u32[]{:S(2)}) collective-permute-start(bf16[8,384,256]{2,1,0:T(8,128)(2,1)S(1)} %all-to-all-done), channel_id=1, source_target_pairs={{0,1},{1,0},{2,3},{3,2},{4,5},{5,4},{6,7},{7,6},{8,9},{9,8},{10,11... | collective-permute-start | bytes 4718600 | tf_op jit(solution)/shard_map/ppermute | solution.py:222
  63.8 15.7 %collective-permute-start.5 = (bf16[384,256]{1,0:T(8,128)(2,1)S(1)}, bf16[384,256]{1,0:T(8,128)(2,1)S(1)}, u32[]{:S(2)}, u32[]{:S(2)}) collective-permute-start(bf16[384,256]{1,0:T(8,128)(2,1)S(1)} %maximum_maximum_fusion.1), channel_id=1, source_target_pairs={{0,8},{8,0},{1,9},{9,1},{2,10},{10,2},{3,11},{11,3},{4,12},{12,4},... | collective-permute-start | bytes 589832 | tf_op jit(solution)/shard_map/ppermute | solution.py:220
  73.9 20.1 %copy-start.1 = (bf16[1,256,2048]{2,1,0:T(8,128)(2,1)S(1)}, bf16[1,256,2048]{2,1,0:T(8,128)(2,1)}, u32[]{:S(2)}) copy-start(bf16[1,256,2048]{2,1,0:T(8,128)(2,1)} %param.5) | copy-start | bytes 3145732
  80.3 28.1 %collective-permute-start.7 = (bf16[2,384,256]{2,1,0:T(8,128)(2,1)}, bf16[2,384,256]{2,1,0:T(8,128)(2,1)}, u32[]{:S(2)}, u32[]{:S(2)}) collective-permute-start(bf16[2,384,256]{2,1,0:T(8,128)(2,1)} %get-tuple-element.31), channel_id=1, source_target_pairs={{0,4},{2,6},{4,0},{6,2},{1,5},{3,7},{5,1},{7,3},{8,12},{10,14},{12... | collective-permute-start | bytes 1179656 | tf_op jit(solution)/shard_map/ppermute | solution.py:224
  85.2 23.2 %collective-permute-start.6 = (bf16[2,384,256]{2,1,0:T(8,128)(2,1)}, bf16[2,384,256]{2,1,0:T(8,128)(2,1)}, u32[]{:S(2)}, u32[]{:S(2)}) collective-permute-start(bf16[2,384,256]{2,1,0:T(8,128)(2,1)} %get-tuple-element.31), channel_id=1, source_target_pairs={{0,2},{2,0},{4,6},{6,4},{1,3},{3,1},{5,7},{7,5},{8,10},{10,8},{12,... | collective-permute-start | bytes 1179656 | tf_op jit(solution)/shard_map/ppermute | solution.py:224
  91.9 16.5 %collective-permute-start.8 = (bf16[2,384,256]{2,1,0:T(8,128)(2,1)}, bf16[2,384,256]{2,1,0:T(8,128)(2,1)}, u32[]{:S(2)}, u32[]{:S(2)}) collective-permute-start(bf16[2,384,256]{2,1,0:T(8,128)(2,1)} %get-tuple-element.31), channel_id=1, source_target_pairs={{0,6},{2,4},{4,2},{6,0},{1,7},{3,5},{5,3},{7,1},{8,14},{10,12},{12... | collective-permute-start | bytes 1179656 | tf_op jit(solution)/shard_map/ppermute | solution.py:224
  96.4 0.8 copy-start
  97.2 27.7 %all-to-all-start.1 = ((bf16[16,8,2048]{2,1,0:T(8,128)(2,1)}), bf16[16,8,2048]{2,1,0:T(8,128)(2,1)S(1)}, u32[]{:S(2)}, u32[]{:S(2)}) async-start(bf16[16,8,2048]{2,1,0:T(8,128)(2,1)} %bitcast.39), calls=%async_computation.1 | async-start | bytes 1048576 | tf_op jit(solution)/shard_map/all_to_all | solution.py:236
  109.8 21.3 %collective-permute-start.9 = (bf16[4,2,384,256]{3,2,1,0:T(8,128)(2,1)S(1)}, bf16[4,2,384,256]{3,2,1,0:T(8,128)(2,1)}, u32[]{:S(2)}, u32[]{:S(2)}) collective-permute-start(bf16[4,2,384,256]{3,2,1,0:T(8,128)(2,1)S(1)} %pad_maximum_fusion.own), channel_id=1, source_target_pairs={{0,1},{1,0},{2,3},{3,2},{4,5},{5,4},{6,7},{7,6},{8,9},{9,8},{10,11... | collective-permute-start | bytes 4718600 | tf_op jit(solution)/shard_map/ppermute | solution.py:226
  125.9 21.7 %all-to-all-start.2 = ((bf16[16,8,2048]{2,1,0:T(8,128)(2,1)}), bf16[16,8,2048]{2,1,0:T(8,128)(2,1)S(1)}, u32[]{:S(2)}, u32[]{:S(2)}) async-start(bf16[16,8,2048]{2,1,0:T(8,128)(2,1)} %get-tuple-element.19), calls=%async_computation.2 | async-start | bytes 1048576 | tf_op jit(solution)/shard_map/all_to_all | solution.py:239

commit v2 on v0

--- a/solution.py
+++ b/solution.py
@@ -95,17 +95,18 @@
                 block = wide[s, x]
                 gate[at : at + 256] = jnp.where(even, block[:, :128], block[:, 128:256])
                 up[at : at + 256] = jnp.where(even, block[:, 256:384], block[:, 384:])
-        for g in range(2):
-            for x in range(4):
-                block = down[g, x]
-                at = 1024 * g + 256 * x
-                served[:, at : at + 256] = jnp.where(even, block[:128], block[128:])
         copies = [
             pltpu.make_async_copy(a, b.at[layer], done.at[i])
             for i, (a, b) in enumerate(((gate, gates), (up, ups), (served, serveds)))
         ]
-        for copy in copies:
+        for copy in copies[:2]:
             copy.start()
+        for g in range(2):
+            for x in range(4):
+                block = down[g, x]
+                at = 1024 * g + 256 * x
+                served[:, at : at + 256] = jnp.where(even, block[:128], block[128:])
+        copies[2].start()
         for s in range(2):
             for x in range(4):
                 at = 1024 * s + 256 * x
@@ -183,8 +184,11 @@
 
 def step(prompt, norm_gain, gate_weight, up_weight, down_weight):
     gain = norm_gain[:, :, None]
-    gate = (gain * gate_weight).astype(bf16)
-    up = (gain * up_weight).astype(bf16)
+    gate = [(gain[0] * gate_weight[0]).astype(bf16)]
+    up = [(gain[0] * up_weight[0]).astype(bf16)]
+    gate[0], up[0], later = lax.optimization_barrier((gate[0], up[0], gain[1]))
+    gate.append((later * gate_weight[1]).astype(bf16))
+    up.append((later * up_weight[1]).astype(bf16))
     high = lax.axis_index("gr") == 1
     moved = []
     for layer in range(2):
@@ -206,12 +210,12 @@
     block = unpacked(*in_order(both, across, high))
 
     own = to_everyone(block, ("x", "yl"), 8)
-    own, moved[1] = lax.optimization_barrier((own, moved[1]))
     both = with_down(1)
     across = lax.ppermute(both, "gr", SWAP)
     block = unpacked(*in_order(both, across, high))
     yl = lax.axis_index("yl")
     came = lax.ppermute(block, "yl", SWAP)
+    own, block = lax.optimization_barrier((own, block))
     other = lax.ppermute(own, "core", SWAP)
     pair = jnp.stack(in_order(block, came, yl == 1))
     late = [lax.ppermute(pair, "x", [(x, x ^ k) for x in range(4)]) for k in (1, 2, 3)]

time: 206 us -> 211 us (1.024)
  the two profiles are of different devices: /device:TPU:18 before, /device:TPU:16 now
where the time goes in v2:
time: 211 us; the launch traced here: 210 us
  starting transfers between devices  82.4 us (39%)
  blocking collectives  56.6 us (27%)
  waiting for transfers between devices  53.7 us (25%)
  Pallas kernels  7.07 us (3%)
  other arithmetic  5.21 us (2%)
  local copies, waits for them, and re-layouts  3.92 us (2%)
    all_to_all x1, blocking collectives, step(): normed = lax.all_to_all(sends, axes, 0, 0, tiled=True).reshape(-1, 2048)  33.8 us
    ppermute x2, starting transfers between devices, step(): across = lax.ppermute(both, 'gr', SWAP)  24.4 us
    all_to_all x1, blocking collectives, step(): lax.all_to_all(part.reshape(16, 8, 2048), ('zl', 'yh'), 0, 0, tiled=True)  22.8 us
    all_to_all x1, waiting for transfers between devices, step(): normed = lax.all_to_all(sends, axes, 0, 0, tiled=True).reshape(-1, 2048)  16.4 us
    ppermute x2, waiting for transfers between devices, step(): moved.append(lax.ppermute(block, AXES, weight_moves()))  14.3 us
    ppermute x3, starting transfers between devices, step(): lax.ppermute(pair, 'x', [(x, x ^ k) for x in range(4)])  13.7 us
    all_to_all x1, waiting for transfers between devices, step(): lax.all_to_all(part.reshape(16, 8, 2048), ('zl', 'yh'), 0, 0, tiled=True)  12.2 us
    all_to_all x1, starting transfers between devices, step(): lax.all_to_all(part.reshape(16, 8, 2048), ('zl', 'yh'), 0, 0, tiled=True)  11.3 us
  transfers between devices with their start and end apart: 13, of which 7 were waited for; matrix products, arithmetic and copies ran while one was open for 2% of the time, Pallas kernels for 1%

profile of v2, /device:TPU:16, one launch (start us, length us, event | category | flops | bytes accessed | tf_op | source)
XLA Modules:
  0.0 209.9 jit_solution(17449779193061239631)
XLA Ops:
  1.4 0.9 fusion.2
  2.4 1.9 collective-permute-start
  4.3 0.9 convert_element_type.22
  5.2 3.7 %collective-permute-done = bf16[128,256]{1,0:T(8,128)(2,1)S(1)} collective-permute-done((bf16[128,256]{1,0:T(8,128)(2,1)S(1)}, bf16[128,256]{1,0:T(8,128)(2,1)S(1)}, u32[]{:S(2)}, u32[]{:S(2)}) %collective-permute-start) | collective-permute-done | bytes 65568 | tf_op jit(solution)/shard_map/ppermute | solution.py:196
  8.9 13.9 %collective-permute-start.1 = (bf16[192,256]{1,0:T(8,128)(2,1)S(1)}, bf16[192,256]{1,0:T(8,128)(2,1)S(1)}, u32[]{:S(2)}, u32[]{:S(2)}) collective-permute-start(bf16[192,256]{1,0:T(8,128)(2,1)S(1)} %maximum_maximum_fusion.2), channel_id=1, source_target_pairs={{0,256},{256,0},{1,257},{257,1},{2,258},{258,2},{3,259},{259,3},{4... | collective-permute-start | bytes 294920 | tf_op jit(solution)/shard_map/ppermute | solution.py:209
  22.9 2.6 %collective-permute-done.1 = bf16[192,256]{1,0:T(8,128)(2,1)S(1)} collective-permute-done((bf16[192,256]{1,0:T(8,128)(2,1)S(1)}, bf16[192,256]{1,0:T(8,128)(2,1)S(1)}, u32[]{:S(2)}, u32[]{:S(2)}) %collective-permute-start.1) | collective-permute-done | bytes 98336 | tf_op jit(solution)/shard_map/ppermute | solution.py:209
  25.6 1.3 broadcast_in_dim.2
  26.9 9.9 %all-to-all-start = ((bf16[8,384,256]{2,1,0:T(8,128)(2,1)}), bf16[8,384,256]{2,1,0:T(8,128)(2,1)S(1)}, u32[]{:S(2)}, u32[]{:S(2)}) async-start(bf16[8,384,256]{2,1,0:T(8,128)(2,1)} %broadcast_in_dim.2), calls=%async_computation | async-start | bytes 3145728 | tf_op jit(solution)/shard_map/all_to_all | solution.py:62
  36.9 1.9 collective-permute-start.2
  38.8 10.6 %collective-permute-done.2 = bf16[128,256]{1,0:T(8,128)(2,1)S(1)} collective-permute-done((bf16[128,256]{1,0:T(8,128)(2,1)S(1)}, bf16[128,256]{1,0:T(8,128)(2,1)S(1)}, u32[]{:S(2)}, u32[]{:S(2)}) %collective-permute-start.2) | collective-permute-done | bytes 65568 | tf_op jit(solution)/shard_map/ppermute | solution.py:196
  49.5 10.5 %collective-permute-start.3 = (bf16[192,256]{1,0:T(8,128)(2,1)S(1)}, bf16[192,256]{1,0:T(8,128)(2,1)S(1)}, u32[]{:S(2)}, u32[]{:S(2)}) collective-permute-start(bf16[192,256]{1,0:T(8,128)(2,1)S(1)} %maximum_maximum_fusion.3), channel_id=1, source_target_pairs={{0,256},{256,0},{1,257},{257,1},{2,258},{258,2},{3,259},{259,3},{4... | collective-permute-start | bytes 294920 | tf_op jit(solution)/shard_map/ppermute | solution.py:214
  60.0 2.6 %collective-permute-done.3 = bf16[192,256]{1,0:T(8,128)(2,1)S(1)} collective-permute-done((bf16[192,256]{1,0:T(8,128)(2,1)S(1)}, bf16[192,256]{1,0:T(8,128)(2,1)S(1)}, u32[]{:S(2)}, u32[]{:S(2)}) %collective-permute-start.3) | collective-permute-done | bytes 98336 | tf_op jit(solution)/shard_map/ppermute | solution.py:214
  62.7 1.9 collective-permute-start.4
  64.6 10.0 %collective-permute-start.5 = (bf16[384,256]{1,0:T(8,128)(2,1)S(1)}, bf16[384,256]{1,0:T(8,128)(2,1)S(1)}, u32[]{:S(2)}, u32[]{:S(2)}) collective-permute-start(bf16[384,256]{1,0:T(8,128)(2,1)S(1)} %maximum_maximum_fusion.1), channel_id=1, source_target_pairs={{0,8},{8,0},{1,9},{9,1},{2,10},{10,2},{3,11},{11,3},{4,12},{12,4},... | collective-permute-start | bytes 589832 | tf_op jit(solution)/shard_map/ppermute | solution.py:217
  74.7 5.5 %collective-permute-done.5 = bf16[384,256]{1,0:T(8,128)(2,1)S(1)} collective-permute-done((bf16[384,256]{1,0:T(8,128)(2,1)S(1)}, bf16[384,256]{1,0:T(8,128)(2,1)S(1)}, u32[]{:S(2)}, u32[]{:S(2)}) %collective-permute-start.5) | collective-permute-done | bytes 196640 | tf_op jit(solution)/shard_map/ppermute | solution.py:217
  80.2 0.8 fusion.4
  81.0 4.9 %collective-permute-start.7 = (bf16[2,384,256]{2,1,0:T(8,128)(2,1)}, bf16[2,384,256]{2,1,0:T(8,128)(2,1)}, u32[]{:S(2)}, u32[]{:S(2)}) collective-permute-start(bf16[2,384,256]{2,1,0:T(8,128)(2,1)} %get-tuple-element.37), channel_id=1, source_target_pairs={{0,4},{2,6},{4,0},{6,2},{1,5},{3,7},{5,1},{7,3},{8,12},{10,14},{12... | collective-permute-start | bytes 1179656 | tf_op jit(solution)/shard_map/ppermute | solution.py:221
  85.9 6.7 %collective-permute-start.6 = (bf16[2,384,256]{2,1,0:T(8,128)(2,1)}, bf16[2,384,256]{2,1,0:T(8,128)(2,1)}, u32[]{:S(2)}, u32[]{:S(2)}) collective-permute-start(bf16[2,384,256]{2,1,0:T(8,128)(2,1)} %get-tuple-element.37), channel_id=1, source_target_pairs={{0,2},{2,0},{4,6},{6,4},{1,3},{3,1},{5,7},{7,5},{8,10},{10,8},{12,... | collective-permute-start | bytes 1179656 | tf_op jit(solution)/shard_map/ppermute | solution.py:221
  92.6 2.1 %collective-permute-start.8 = (bf16[2,384,256]{2,1,0:T(8,128)(2,1)}, bf16[2,384,256]{2,1,0:T(8,128)(2,1)}, u32[]{:S(2)}, u32[]{:S(2)}) collective-permute-start(bf16[2,384,256]{2,1,0:T(8,128)(2,1)} %get-tuple-element.37), channel_id=1, source_target_pairs={{0,6},{2,4},{4,2},{6,0},{1,7},{3,5},{5,3},{7,1},{8,14},{10,12},{12... | collective-permute-start | bytes 1179656 | tf_op jit(solution)/shard_map/ppermute | solution.py:221
  95.0 1.6 early_layer.1
  97.4 11.3 %all-to-all-start.1 = ((bf16[16,8,2048]{2,1,0:T(8,128)(2,1)}), bf16[16,8,2048]{2,1,0:T(8,128)(2,1)S(1)}, u32[]{:S(2)}, u32[]{:S(2)}) async-start(bf16[16,8,2048]{2,1,0:T(8,128)(2,1)} %bitcast.52), calls=%async_computation.1 | async-start | bytes 1048576 | tf_op jit(solution)/shard_map/all_to_all | solution.py:233
  108.8 1.4 pad_maximum_fusion.own
  110.2 1.9 collective-permute-start.9
  112.1 0.9 bitcast_convert_fusion.mine
  113.0 12.2 %all-to-all-done.1.parts = bf16[16,8,2048]{2,1,0:T(8,128)(2,1)S(1)} async-done(((bf16[16,8,2048]{2,1,0:T(8,128)(2,1)}), bf16[16,8,2048]{2,1,0:T(8,128)(2,1)S(1)}, u32[]{:S(2)}, u32[]{:S(2)}) %all-to-all-start.1) | async-done | bytes 524320 | tf_op jit(solution)/shard_map/all_to_all | solution.py:233
  125.2 1.0 fold.2
  126.2 5.3 %all-to-all-start.2 = ((bf16[16,8,2048]{2,1,0:T(8,128)(2,1)}), bf16[16,8,2048]{2,1,0:T(8,128)(2,1)S(1)}, u32[]{:S(2)}, u32[]{:S(2)}) async-start(bf16[16,8,2048]{2,1,0:T(8,128)(2,1)} %get-tuple-element.25), calls=%async_computation.2 | async-start | bytes 1048576 | tf_op jit(solution)/shard_map/all_to_all | solution.py:236
  131.5 16.4 %all-to-all-done.2 = bf16[16,8,2048]{2,1,0:T(8,128)(2,1)S(1)} async-done(((bf16[16,8,2048]{2,1,0:T(8,128)(2,1)}), bf16[16,8,2048]{2,1,0:T(8,128)(2,1)S(1)}, u32[]{:S(2)}, u32[]{:S(2)}) %all-to-all-start.2) | async-done | bytes 524320 | tf_op jit(solution)/shard_map/all_to_all | solution.py:236
  148.0 3.5 %late_layer.1 = (bf16[2,2048,128]{2,1,0:T(8,128)(2,1)}, bf16[2,2048,128]{2,1,0:T(8,128)(2,1)}, bf16[2,128,2048]{2,1,0:T(8,128)(2,1)}, bf16[128,2048]{1,0:T(8,128)(2,1)S(1)}) custom-call(bf16[128,2048]{1,0:T(8,128)(2,1)S(1)} %bitcast.50, bf16[4,2,384,256]{3,2,1,0:T(8,128)(2,1)S(1)} %pad_maximum_fusion.own, ...), custom_call_target="tpu_custom_call", output_to_operand_aliasing={{0}: (3, {}), {1}: (4, {}), {2}: (5, {})} | custom-call | tf_op jit(solution)/shard_map/late_layer/pallas_call | solution.py:130
  151.5 22.8 %all_to_all.25.parts = bf16[16,8,2048]{2,1,0:T(8,128)(2,1)S(1)} all-to-all(bf16[16,8,2048]{2,1,0:T(8,128)(2,1)S(1)} %bitcast.53), channel_id=1, replica_groups=mesh['gr'=2,'zl'=4,'yh'=4,'yl'=2,'x'=4,'core'=2] {'zl','yh'}, dimensions={0} | all-to-all | bytes 1048576 | tf_op jit(solution)/shard_map/all_to_all | solution.py:233
  175.1 33.8 %all_to_all.26 = bf16[32,8,2048]{2,1,0:T(8,128)(2,1)S(1)} all-to-all(bf16[32,8,2048]{2,1,0:T(8,128)(2,1)S(1)} %get-tuple-element.35), channel_id=1, replica_groups=mesh['gr'=2,'zl'=4,'yh'=4,'yl'=2,'x'=4,'core'=2] {'yl','zl','yh'}, dimensions={0} | all-to-all | bytes 2097152 | tf_op jit(solution)/shard_map/all_to_all | solution.py:236
  208.9 1.0 copy.16
  (35 shorter events, 2.9 us)
Async XLA Ops:
  2.4 6.5 %collective-permute-start = (bf16[128,256]{1,0:T(8,128)(2,1)S(1)}, bf16[128,256]{1,0:T(8,128)(2,1)S(1)}, u32[]{:S(2)}, u32[]{:S(2)}) collective-permute-start(bf16[128,256]{1,0:T(8,128)(2,1)S(1)} %pad_maximum_fusion.2), channel_id=1, source_target_pairs={{0,0},{1,16},{2,32},{3,48},{4,64},{5,80},{6,96},{7,112},{8,8},{9,2... | collective-permute-start | bytes 196616 | tf_op jit(solution)/shard_map/ppermute | solution.py:196
  8.9 16.5 %collective-permute-start.1 = (bf16[192,256]{1,0:T(8,128)(2,1)S(1)}, bf16[192,256]{1,0:T(8,128)(2,1)S(1)}, u32[]{:S(2)}, u32[]{:S(2)}) collective-permute-start(bf16[192,256]{1,0:T(8,128)(2,1)S(1)} %maximum_maximum_fusion.2), channel_id=1, source_target_pairs={{0,256},{256,0},{1,257},{257,1},{2,258},{258,2},{3,259},{259,3},{4... | collective-permute-start | bytes 294920 | tf_op jit(solution)/shard_map/ppermute | solution.py:209
  26.9 9.9 %copy-start.2 = (f32[2,64,256]{2,1,0:T(8,128)S(1)}, f32[2,64,256]{2,1,0:T(8,128)}, u32[]{:S(2)}) copy-start(f32[2,64,256]{2,1,0:T(8,128)} %param.8) | copy-start | bytes 393220
  26.9 10.0 %copy-start.3 = (f32[2,64,256]{2,1,0:T(8,128)S(1)}, f32[2,64,256]{2,1,0:T(8,128)}, u32[]{:S(2)}) copy-start(f32[2,64,256]{2,1,0:T(8,128)} %param.7) | copy-start | bytes 393220
  26.9 35.8 %all-to-all-start = ((bf16[8,384,256]{2,1,0:T(8,128)(2,1)}), bf16[8,384,256]{2,1,0:T(8,128)(2,1)S(1)}, u32[]{:S(2)}, u32[]{:S(2)}) async-start(bf16[8,384,256]{2,1,0:T(8,128)(2,1)} %broadcast_in_dim.2), calls=%async_computation | async-start | bytes 3145728 | tf_op jit(solution)/shard_map/all_to_all | solution.py:62
  36.9 12.5 %collective-permute-start.2 = (bf16[128,256]{1,0:T(8,128)(2,1)S(1)}, bf16[128,256]{1,0:T(8,128)(2,1)S(1)}, u32[]{:S(2)}, u32[]{:S(2)}) collective-permute-start(bf16[128,256]{1,0:T(8,128)(2,1)S(1)} %pad_maximum_fusion.3), channel_id=1, source_target_pairs={{0,0},{1,16},{2,32},{3,48},{4,64},{5,80},{6,96},{7,112},{8,8},{9,2... | collective-permute-start | bytes 196616 | tf_op jit(solution)/shard_map/ppermute | solution.py:196
  49.5 13.1 %collective-permute-start.3 = (bf16[192,256]{1,0:T(8,128)(2,1)S(1)}, bf16[192,256]{1,0:T(8,128)(2,1)S(1)}, u32[]{:S(2)}, u32[]{:S(2)}) collective-permute-start(bf16[192,256]{1,0:T(8,128)(2,1)S(1)} %maximum_maximum_fusion.3), channel_id=1, source_target_pairs={{0,256},{256,0},{1,257},{257,1},{2,258},{258,2},{3,259},{259,3},{4... | collective-permute-start | bytes 294920 | tf_op jit(solution)/shard_map/ppermute | solution.py:214
  62.7 32.3 %collective-permute-start.4 = (bf16[8,384,256]{2,1,0:T(8,128)(2,1)S(1)}, bf16[8,384,256]{2,1,0:T(8,128)(2,1)S(1)}, u32[]{:S(2)}, u32[]{:S(2)}) collective-permute-start(bf16[8,384,256]{2,1,0:T(8,128)(2,1)S(1)} %all-to-all-done), channel_id=1, source_target_pairs={{0,1},{1,0},{2,3},{3,2},{4,5},{5,4},{6,7},{7,6},{8,9},{9,8},{10,11... | collective-permute-start | bytes 4718600 | tf_op jit(solution)/shard_map/ppermute | solution.py:219
  64.6 15.6 %collective-permute-start.5 = (bf16[384,256]{1,0:T(8,128)(2,1)S(1)}, bf16[384,256]{1,0:T(8,128)(2,1)S(1)}, u32[]{:S(2)}, u32[]{:S(2)}) collective-permute-start(bf16[384,256]{1,0:T(8,128)(2,1)S(1)} %maximum_maximum_fusion.1), channel_id=1, source_target_pairs={{0,8},{8,0},{1,9},{9,1},{2,10},{10,2},{3,11},{11,3},{4,12},{12,4},... | collective-permute-start | bytes 589832 | tf_op jit(solution)/shard_map/ppermute | solution.py:217
  74.7 20.1 %copy-start.1 = (bf16[1,256,2048]{2,1,0:T(8,128)(2,1)S(1)}, bf16[1,256,2048]{2,1,0:T(8,128)(2,1)}, u32[]{:S(2)}) copy-start(bf16[1,256,2048]{2,1,0:T(8,128)(2,1)} %param.5) | copy-start | bytes 3145732
  81.0 27.7 %collective-permute-start.7 = (bf16[2,384,256]{2,1,0:T(8,128)(2,1)}, bf16[2,384,256]{2,1,0:T(8,128)(2,1)}, u32[]{:S(2)}, u32[]{:S(2)}) collective-permute-start(bf16[2,384,256]{2,1,0:T(8,128)(2,1)} %get-tuple-element.37), channel_id=1, source_target_pairs={{0,4},{2,6},{4,0},{6,2},{1,5},{3,7},{5,1},{7,3},{8,12},{10,14},{12... | collective-permute-start | bytes 1179656 | tf_op jit(solution)/shard_map/ppermute | solution.py:221
  85.9 22.8 %collective-permute-start.6 = (bf16[2,384,256]{2,1,0:T(8,128)(2,1)}, bf16[2,384,256]{2,1,0:T(8,128)(2,1)}, u32[]{:S(2)}, u32[]{:S(2)}) collective-permute-start(bf16[2,384,256]{2,1,0:T(8,128)(2,1)} %get-tuple-element.37), channel_id=1, source_target_pairs={{0,2},{2,0},{4,6},{6,4},{1,3},{3,1},{5,7},{7,5},{8,10},{10,8},{12,... | collective-permute-start | bytes 1179656 | tf_op jit(solution)/shard_map/ppermute | solution.py:221
  92.6 16.1 %collective-permute-start.8 = (bf16[2,384,256]{2,1,0:T(8,128)(2,1)}, bf16[2,384,256]{2,1,0:T(8,128)(2,1)}, u32[]{:S(2)}, u32[]{:S(2)}) collective-permute-start(bf16[2,384,256]{2,1,0:T(8,128)(2,1)} %get-tuple-element.37), channel_id=1, source_target_pairs={{0,6},{2,4},{4,2},{6,0},{1,7},{3,5},{5,3},{7,1},{8,14},{10,12},{12... | collective-permute-start | bytes 1179656 | tf_op jit(solution)/shard_map/ppermute | solution.py:221
  96.7 0.8 copy-start
  97.4 27.8 %all-to-all-start.1 = ((bf16[16,8,2048]{2,1,0:T(8,128)(2,1)}), bf16[16,8,2048]{2,1,0:T(8,128)(2,1)S(1)}, u32[]{:S(2)}, u32[]{:S(2)}) async-start(bf16[16,8,2048]{2,1,0:T(8,128)(2,1)} %bitcast.52), calls=%async_computation.1 | async-start | bytes 1048576 | tf_op jit(solution)/shard_map/all_to_all | solution.py:233
  110.2 21.3 %collective-permute-start.9 = (bf16[4,2,384,256]{3,2,1,0:T(8,128)(2,1)S(1)}, bf16[4,2,384,256]{3,2,1,0:T(8,128)(2,1)}, u32[]{:S(2)}, u32[]{:S(2)}) collective-permute-start(bf16[4,2,384,256]{3,2,1,0:T(8,128)(2,1)S(1)} %pad_maximum_fusion.own), channel_id=1, source_target_pairs={{0,1},{1,0},{2,3},{3,2},{4,5},{5,4},{6,7},{7,6},{8,9},{9,8},{10,11... | collective-permute-start | bytes 4718600 | tf_op jit(solution)/shard_map/ppermute | solution.py:223
  126.2 21.7 %all-to-all-start.2 = ((bf16[16,8,2048]{2,1,0:T(8,128)(2,1)}), bf16[16,8,2048]{2,1,0:T(8,128)(2,1)S(1)}, u32[]{:S(2)}, u32[]{:S(2)}) async-start(bf16[16,8,2048]{2,1,0:T(8,128)(2,1)} %get-tuple-element.25), calls=%async_computation.2 | async-start | bytes 1048576 | tf_op jit(solution)/shard_map/all_to_all | solution.py:236

commit v3 on v0

--- a/solution.py
+++ b/solution.py
@@ -206,12 +206,12 @@
     block = unpacked(*in_order(both, across, high))
 
     own = to_everyone(block, ("x", "yl"), 8)
-    own, moved[1] = lax.optimization_barrier((own, moved[1]))
     both = with_down(1)
     across = lax.ppermute(both, "gr", SWAP)
     block = unpacked(*in_order(both, across, high))
     yl = lax.axis_index("yl")
     came = lax.ppermute(block, "yl", SWAP)
+    own, block = lax.optimization_barrier((own, block))
     other = lax.ppermute(own, "core", SWAP)
     pair = jnp.stack(in_order(block, came, yl == 1))
     late = [lax.ppermute(pair, "x", [(x, x ^ k) for x in range(4)]) for k in (1, 2, 3)]
@@ -219,16 +219,16 @@
     late_other = lax.ppermute(late, "core", SWAP)
 
     half = lax.dynamic_slice_in_dim(prompt[0], yl * 128, 128, 0)
-    mine = lax.dynamic_slice_in_dim(half, lax.axis_index(("zl", "yh")) * 8, 8, 0).astype(f32)
+    mine = lax.dynamic_slice_in_dim(half, lax.axis_index(("yh", "zl")) * 8, 8, 0).astype(f32)
     normed = norm_call(half)
     early = [a.reshape(4, 2, 384, 256) for a in (own, other)]
     outputs = ()
     for layer in range(2):
         pieces = (late, late_other) if layer else early
         *outputs, part = layer_call(layer == 1, normed, *pieces, outputs)
-        parts = lax.all_to_all(part.reshape(16, 8, 2048), ("zl", "yh"), 0, 0, tiled=True)
+        parts = lax.all_to_all(part.reshape(16, 8, 2048), ("yh", "zl"), 0, 0, tiled=True)
         sends, mine = fold_call(layer == 1, parts, mine)
-        axes = ("yl", "zl", "yh") if layer else ("zl", "yh")
+        axes = ("yl", "yh", "zl") if layer else ("yh", "zl")
         normed = lax.all_to_all(sends, axes, 0, 0, tiled=True).reshape(-1, 2048)
     return *outputs, normed.reshape(prompt.shape)
 

time: 206 us -> 211 us (1.024)
  the two profiles are of different devices: /device:TPU:18 before, /device:TPU:8 now
where the time goes in v3:
time: 211 us; the launch traced here: 210 us
  starting transfers between devices  91.5 us (43%)
  blocking collectives  60.8 us (29%)
  waiting for transfers between devices  41.2 us (20%)
  Pallas kernels  7.08 us (3%)
  other arithmetic  5.26 us (2%)
  local copies, waits for them, and re-layouts  3.16 us (1%)
    all_to_all x1, blocking collectives, step(): normed = lax.all_to_all(sends, axes, 0, 0, tiled=True).reshape(-1, 2048)  38.9 us
    ppermute x2, starting transfers between devices, step(): across = lax.ppermute(both, 'gr', SWAP)  33.7 us
    all_to_all x1, blocking collectives, step(): lax.all_to_all(part.reshape(16, 8, 2048), ('yh', 'zl'), 0, 0, tiled=True)  21.9 us
    all_to_all x1, waiting for transfers between devices, step(): normed = lax.all_to_all(sends, axes, 0, 0, tiled=True).reshape(-1, 2048)  15.7 us
    ppermute x1, starting transfers between devices, step(): other = lax.ppermute(own, 'core', SWAP)  12.4 us
    ppermute x3, starting transfers between devices, step(): lax.ppermute(pair, 'x', [(x, x ^ k) for x in range(4)])  12.3 us
    all_to_all x1, starting transfers between devices, to_everyone(): lax.all_to_all(jnp.broadcast_to(value[None], (count, *value.shape)), axes...  11.5 us
    all_to_all x1, starting transfers between devices, step(): lax.all_to_all(part.reshape(16, 8, 2048), ('yh', 'zl'), 0, 0, tiled=True)  10.1 us
  transfers between devices with their start and end apart: 13, of which 6 were waited for; matrix products, arithmetic and copies ran while one was open for 2% of the time, Pallas kernels for 1%

profile of v3, /device:TPU:8, one launch (start us, length us, event | category | flops | bytes accessed | tf_op | source)
XLA Modules:
  0.0 210.0 jit_solution(7098509848520342720)
XLA Ops:
  0.6 1.1 multiply_convert_fusion.1
  1.7 0.7 collective-permute-start
  2.4 0.9 convert_element_type.16
  3.4 17.6 %collective-permute-start.1 = (bf16[192,256]{1,0:T(8,128)(2,1)S(1)}, bf16[192,256]{1,0:T(8,128)(2,1)S(1)}, u32[]{:S(2)}, u32[]{:S(2)}) collective-permute-start(bf16[192,256]{1,0:T(8,128)(2,1)S(1)} %maximum_maximum_fusion.2), channel_id=1, source_target_pairs={{0,256},{256,0},{1,257},{257,1},{2,258},{258,2},{3,259},{259,3},{4... | collective-permute-start | bytes 294920 | tf_op jit(solution)/shard_map/ppermute | solution.py:205
  21.0 4.9 %collective-permute-done.1 = bf16[192,256]{1,0:T(8,128)(2,1)S(1)} collective-permute-done((bf16[192,256]{1,0:T(8,128)(2,1)S(1)}, bf16[192,256]{1,0:T(8,128)(2,1)S(1)}, u32[]{:S(2)}, u32[]{:S(2)}) %collective-permute-start.1) | collective-permute-done | bytes 98336 | tf_op jit(solution)/shard_map/ppermute | solution.py:205
  26.0 1.3 broadcast_in_dim.2
  27.3 11.5 %all-to-all-start = ((bf16[8,384,256]{2,1,0:T(8,128)(2,1)}), bf16[8,384,256]{2,1,0:T(8,128)(2,1)S(1)}, u32[]{:S(2)}, u32[]{:S(2)}) async-start(bf16[8,384,256]{2,1,0:T(8,128)(2,1)} %broadcast_in_dim.2), calls=%async_computation | async-start | bytes 3145728 | tf_op jit(solution)/shard_map/all_to_all | solution.py:62
  39.6 16.1 %collective-permute-start.3 = (bf16[192,256]{1,0:T(8,128)(2,1)S(1)}, bf16[192,256]{1,0:T(8,128)(2,1)S(1)}, u32[]{:S(2)}, u32[]{:S(2)}) collective-permute-start(bf16[192,256]{1,0:T(8,128)(2,1)S(1)} %maximum_maximum_fusion.3), channel_id=1, source_target_pairs={{0,256},{256,0},{1,257},{257,1},{2,258},{258,2},{3,259},{259,3},{4... | collective-permute-start | bytes 294920 | tf_op jit(solution)/shard_map/ppermute | solution.py:210
  55.7 3.4 %collective-permute-done.3 = bf16[192,256]{1,0:T(8,128)(2,1)S(1)} collective-permute-done((bf16[192,256]{1,0:T(8,128)(2,1)S(1)}, bf16[192,256]{1,0:T(8,128)(2,1)S(1)}, u32[]{:S(2)}, u32[]{:S(2)}) %collective-permute-start.3) | collective-permute-done | bytes 98336 | tf_op jit(solution)/shard_map/ppermute | solution.py:210
  59.3 12.4 %collective-permute-start.4 = (bf16[8,384,256]{2,1,0:T(8,128)(2,1)S(1)}, bf16[8,384,256]{2,1,0:T(8,128)(2,1)S(1)}, u32[]{:S(2)}, u32[]{:S(2)}) collective-permute-start(bf16[8,384,256]{2,1,0:T(8,128)(2,1)S(1)} %all-to-all-done), channel_id=1, source_target_pairs={{0,1},{1,0},{2,3},{3,2},{4,5},{5,4},{6,7},{7,6},{8,9},{9,8},{10,11... | collective-permute-start | bytes 4718600 | tf_op jit(solution)/shard_map/ppermute | solution.py:215
  71.7 1.9 collective-permute-start.5
  73.6 6.8 %collective-permute-done.5 = bf16[384,256]{1,0:T(8,128)(2,1)S(1)} collective-permute-done((bf16[384,256]{1,0:T(8,128)(2,1)S(1)}, bf16[384,256]{1,0:T(8,128)(2,1)S(1)}, u32[]{:S(2)}, u32[]{:S(2)}) %collective-permute-start.5) | collective-permute-done | bytes 196640 | tf_op jit(solution)/shard_map/ppermute | solution.py:213
  80.4 0.8 fusion
  81.2 4.5 %collective-permute-start.7 = (bf16[2,384,256]{2,1,0:T(8,128)(2,1)}, bf16[2,384,256]{2,1,0:T(8,128)(2,1)}, u32[]{:S(2)}, u32[]{:S(2)}) collective-permute-start(bf16[2,384,256]{2,1,0:T(8,128)(2,1)} %get-tuple-element.31), channel_id=1, source_target_pairs={{0,4},{2,6},{4,0},{6,2},{1,5},{3,7},{5,1},{7,3},{8,12},{10,14},{12... | collective-permute-start | bytes 1179656 | tf_op jit(solution)/shard_map/ppermute | solution.py:217
  85.7 5.9 %collective-permute-start.6 = (bf16[2,384,256]{2,1,0:T(8,128)(2,1)}, bf16[2,384,256]{2,1,0:T(8,128)(2,1)}, u32[]{:S(2)}, u32[]{:S(2)}) collective-permute-start(bf16[2,384,256]{2,1,0:T(8,128)(2,1)} %get-tuple-element.31), channel_id=1, source_target_pairs={{0,2},{2,0},{4,6},{6,4},{1,3},{3,1},{5,7},{7,5},{8,10},{10,8},{12,... | collective-permute-start | bytes 1179656 | tf_op jit(solution)/shard_map/ppermute | solution.py:217
  91.6 1.9 collective-permute-start.8
  93.8 1.6 early_layer.1
  95.5 0.8 copy-done
  96.2 10.1 %all-to-all-start.1 = ((bf16[16,8,2048]{2,1,0:T(8,128)(2,1)}), bf16[16,8,2048]{2,1,0:T(8,128)(2,1)S(1)}, u32[]{:S(2)}, u32[]{:S(2)}) async-start(bf16[16,8,2048]{2,1,0:T(8,128)(2,1)} %bitcast.39), calls=%async_computation.1 | async-start | bytes 1048576 | tf_op jit(solution)/shard_map/all_to_all | solution.py:229
  106.4 0.7 collective-permute-done.6
  107.1 1.4 pad_maximum_fusion.own
  108.5 1.9 collective-permute-start.9
  110.5 0.9 bitcast_convert_fusion.mine
  111.4 9.7 %all-to-all-done.1.parts = bf16[16,8,2048]{2,1,0:T(8,128)(2,1)S(1)} async-done(((bf16[16,8,2048]{2,1,0:T(8,128)(2,1)}), bf16[16,8,2048]{2,1,0:T(8,128)(2,1)S(1)}, u32[]{:S(2)}, u32[]{:S(2)}) %all-to-all-start.1) | async-done | bytes 524320 | tf_op jit(solution)/shard_map/all_to_all | solution.py:229
  121.0 1.0 fold.2
  122.0 6.3 %all-to-all-start.2 = ((bf16[16,8,2048]{2,1,0:T(8,128)(2,1)}), bf16[16,8,2048]{2,1,0:T(8,128)(2,1)S(1)}, u32[]{:S(2)}, u32[]{:S(2)}) async-start(bf16[16,8,2048]{2,1,0:T(8,128)(2,1)} %get-tuple-element.19), calls=%async_computation.2 | async-start | bytes 1048576 | tf_op jit(solution)/shard_map/all_to_all | solution.py:232
  128.3 15.7 %all-to-all-done.2 = bf16[16,8,2048]{2,1,0:T(8,128)(2,1)S(1)} async-done(((bf16[16,8,2048]{2,1,0:T(8,128)(2,1)}), bf16[16,8,2048]{2,1,0:T(8,128)(2,1)S(1)}, u32[]{:S(2)}, u32[]{:S(2)}) %all-to-all-start.2) | async-done | bytes 524320 | tf_op jit(solution)/shard_map/all_to_all | solution.py:232
  144.0 3.5 %late_layer.1 = (bf16[2,2048,128]{2,1,0:T(8,128)(2,1)}, bf16[2,2048,128]{2,1,0:T(8,128)(2,1)}, bf16[2,128,2048]{2,1,0:T(8,128)(2,1)}, bf16[128,2048]{1,0:T(8,128)(2,1)S(1)}) custom-call(bf16[128,2048]{1,0:T(8,128)(2,1)S(1)} %bitcast.37, bf16[4,2,384,256]{3,2,1,0:T(8,128)(2,1)S(1)} %pad_maximum_fusion.own, ...), custom_call_target="tpu_custom_call", output_to_operand_aliasing={{0}: (3, {}), {1}: (4, {}), {2}: (5, {})} | custom-call | tf_op jit(solution)/shard_map/late_layer/pallas_call | solution.py:129
  147.5 21.9 %all_to_all.25.parts = bf16[16,8,2048]{2,1,0:T(8,128)(2,1)S(1)} all-to-all(bf16[16,8,2048]{2,1,0:T(8,128)(2,1)S(1)} %bitcast.40), channel_id=1, replica_groups=mesh['gr'=2,'zl'=4,'yh'=4,'yl'=2,'x'=4,'core'=2] {'yh','zl'}, dimensions={0} | all-to-all | bytes 1048576 | tf_op jit(solution)/shard_map/all_to_all | solution.py:229
  169.4 0.8 fold.3
  170.2 38.9 %all_to_all.26 = bf16[32,8,2048]{2,1,0:T(8,128)(2,1)S(1)} all-to-all(bf16[32,8,2048]{2,1,0:T(8,128)(2,1)S(1)} %get-tuple-element.29), channel_id=1, replica_groups=mesh['gr'=2,'zl'=4,'yh'=4,'yl'=2,'x'=4,'core'=2] {'yl','yh','zl'}, dimensions={0} | all-to-all | bytes 2097152 | tf_op jit(solution)/shard_map/all_to_all | solution.py:232
  209.1 1.0 copy.16
  (32 shorter events, 1.2 us)
Async XLA Ops:
  1.7 1.6 collective-permute-start
  3.4 22.5 %collective-permute-start.1 = (bf16[192,256]{1,0:T(8,128)(2,1)S(1)}, bf16[192,256]{1,0:T(8,128)(2,1)S(1)}, u32[]{:S(2)}, u32[]{:S(2)}) collective-permute-start(bf16[192,256]{1,0:T(8,128)(2,1)S(1)} %maximum_maximum_fusion.2), channel_id=1, source_target_pairs={{0,256},{256,0},{1,257},{257,1},{2,258},{258,2},{3,259},{259,3},{4... | collective-permute-start | bytes 294920 | tf_op jit(solution)/shard_map/ppermute | solution.py:205
  27.3 32.0 %all-to-all-start = ((bf16[8,384,256]{2,1,0:T(8,128)(2,1)}), bf16[8,384,256]{2,1,0:T(8,128)(2,1)S(1)}, u32[]{:S(2)}, u32[]{:S(2)}) async-start(bf16[8,384,256]{2,1,0:T(8,128)(2,1)} %broadcast_in_dim.2), calls=%async_computation | async-start | bytes 3145728 | tf_op jit(solution)/shard_map/all_to_all | solution.py:62
  38.9 0.7 collective-permute-start.2
  39.6 19.6 %collective-permute-start.3 = (bf16[192,256]{1,0:T(8,128)(2,1)S(1)}, bf16[192,256]{1,0:T(8,128)(2,1)S(1)}, u32[]{:S(2)}, u32[]{:S(2)}) collective-permute-start(bf16[192,256]{1,0:T(8,128)(2,1)S(1)} %maximum_maximum_fusion.3), channel_id=1, source_target_pairs={{0,256},{256,0},{1,257},{257,1},{2,258},{258,2},{3,259},{259,3},{4... | collective-permute-start | bytes 294920 | tf_op jit(solution)/shard_map/ppermute | solution.py:210
  59.3 34.6 %collective-permute-start.4 = (bf16[8,384,256]{2,1,0:T(8,128)(2,1)S(1)}, bf16[8,384,256]{2,1,0:T(8,128)(2,1)S(1)}, u32[]{:S(2)}, u32[]{:S(2)}) collective-permute-start(bf16[8,384,256]{2,1,0:T(8,128)(2,1)S(1)} %all-to-all-done), channel_id=1, source_target_pairs={{0,1},{1,0},{2,3},{3,2},{4,5},{5,4},{6,7},{7,6},{8,9},{9,8},{10,11... | collective-permute-start | bytes 4718600 | tf_op jit(solution)/shard_map/ppermute | solution.py:215
  71.7 8.7 %collective-permute-start.5 = (bf16[384,256]{1,0:T(8,128)(2,1)S(1)}, bf16[384,256]{1,0:T(8,128)(2,1)S(1)}, u32[]{:S(2)}, u32[]{:S(2)}) collective-permute-start(bf16[384,256]{1,0:T(8,128)(2,1)S(1)} %maximum_maximum_fusion.1), channel_id=1, source_target_pairs={{0,8},{8,0},{1,9},{9,1},{2,10},{10,2},{3,11},{11,3},{4,12},{12,4},... | collective-permute-start | bytes 589832 | tf_op jit(solution)/shard_map/ppermute | solution.py:213
  73.6 20.0 %copy-start.1 = (bf16[1,256,2048]{2,1,0:T(8,128)(2,1)S(1)}, bf16[1,256,2048]{2,1,0:T(8,128)(2,1)}, u32[]{:S(2)}) copy-start(bf16[1,256,2048]{2,1,0:T(8,128)(2,1)} %param.5) | copy-start | bytes 3145732
  81.2 25.1 %collective-permute-start.7 = (bf16[2,384,256]{2,1,0:T(8,128)(2,1)}, bf16[2,384,256]{2,1,0:T(8,128)(2,1)}, u32[]{:S(2)}, u32[]{:S(2)}) collective-permute-start(bf16[2,384,256]{2,1,0:T(8,128)(2,1)} %get-tuple-element.31), channel_id=1, source_target_pairs={{0,4},{2,6},{4,0},{6,2},{1,5},{3,7},{5,1},{7,3},{8,12},{10,14},{12... | collective-permute-start | bytes 1179656 | tf_op jit(solution)/shard_map/ppermute | solution.py:217
  85.7 21.4 %collective-permute-start.6 = (bf16[2,384,256]{2,1,0:T(8,128)(2,1)}, bf16[2,384,256]{2,1,0:T(8,128)(2,1)}, u32[]{:S(2)}, u32[]{:S(2)}) collective-permute-start(bf16[2,384,256]{2,1,0:T(8,128)(2,1)} %get-tuple-element.31), channel_id=1, source_target_pairs={{0,2},{2,0},{4,6},{6,4},{1,3},{3,1},{5,7},{7,5},{8,10},{10,8},{12,... | collective-permute-start | bytes 1179656 | tf_op jit(solution)/shard_map/ppermute | solution.py:217
  91.6 15.5 %collective-permute-start.8 = (bf16[2,384,256]{2,1,0:T(8,128)(2,1)}, bf16[2,384,256]{2,1,0:T(8,128)(2,1)}, u32[]{:S(2)}, u32[]{:S(2)}) collective-permute-start(bf16[2,384,256]{2,1,0:T(8,128)(2,1)} %get-tuple-element.31), channel_id=1, source_target_pairs={{0,6},{2,4},{4,2},{6,0},{1,7},{3,5},{5,3},{7,1},{8,14},{10,12},{12... | collective-permute-start | bytes 1179656 | tf_op jit(solution)/shard_map/ppermute | solution.py:217
  95.4 0.8 copy-start
  96.2 24.8 %all-to-all-start.1 = ((bf16[16,8,2048]{2,1,0:T(8,128)(2,1)}), bf16[16,8,2048]{2,1,0:T(8,128)(2,1)S(1)}, u32[]{:S(2)}, u32[]{:S(2)}) async-start(bf16[16,8,2048]{2,1,0:T(8,128)(2,1)} %bitcast.39), calls=%async_computation.1 | async-start | bytes 1048576 | tf_op jit(solution)/shard_map/all_to_all | solution.py:229
  108.5 19.8 %collective-permute-start.9 = (bf16[4,2,384,256]{3,2,1,0:T(8,128)(2,1)S(1)}, bf16[4,2,384,256]{3,2,1,0:T(8,128)(2,1)}, u32[]{:S(2)}, u32[]{:S(2)}) collective-permute-start(bf16[4,2,384,256]{3,2,1,0:T(8,128)(2,1)S(1)} %pad_maximum_fusion.own), channel_id=1, source_target_pairs={{0,1},{1,0},{2,3},{3,2},{4,5},{5,4},{6,7},{7,6},{8,9},{9,8},{10,11... | collective-permute-start | bytes 4718600 | tf_op jit(solution)/shard_map/ppermute | solution.py:219
  122.0 21.9 %all-to-all-start.2 = ((bf16[16,8,2048]{2,1,0:T(8,128)(2,1)}), bf16[16,8,2048]{2,1,0:T(8,128)(2,1)S(1)}, u32[]{:S(2)}, u32[]{:S(2)}) async-start(bf16[16,8,2048]{2,1,0:T(8,128)(2,1)} %get-tuple-element.19), calls=%async_computation.2 | async-start | bytes 1048576 | tf_op jit(solution)/shard_map/all_to_all | solution.py:232
